TPU v7x, 128 devices: a whole 4x4x4 slice. The times are simulated.
128 devices in a mesh: ep: 32 (over z, y, core), tp: 4 (over x).
Axes of the slice: x: 4, y: 4, z: 4, core: 2. Of those that a mesh axis runs over, the one named last changes fastest.
Arguments:
- mixer_value: bfloat16 [16384, 2048], P('ep', 'tp'), may hold values from -1 to 2
- mixer_gate: bfloat16 [16384, 2048], P('ep', 'tp'), may hold values from -6 to 6
- mixer_taps: bfloat16 [31, 2048], P(None, 'tp'), may hold values from -60 to 60
- mixer_gain: bfloat16 [2048], P('tp'), may hold values from 0.099609375 to 1.8984375
- mixer_weight: bfloat16 [2048, 4096], P('tp'), may hold values from -0.125 to 0.125
- routed_input: bfloat16 [16384, 4096], P('ep'), may hold values from -6 to 6
- routed_gain: bfloat16 [4096], replicated, may hold values from 0.099609375 to 1.8984375
- expert_ids: int32 [16384, 2], P('ep'), may hold values from 0 to 31, all different within a row; in each aligned block of 128 rows (0 to 127, 128 to 255, ...) at most 10 rows name the same one
- route_share: float32 [16384, 2], P('ep'), may hold values from 0.2 to 1
- gate_weight: bfloat16 [32, 4096, 2048], P('ep', None, 'tp'), may hold values from -0.09375 to 0.09375
- up_weight: bfloat16 [32, 4096, 2048], P('ep', None, 'tp'), may hold values from -0.09375 to 0.09375
- down_weight: bfloat16 [32, 2048, 4096], P('ep', 'tp'), may hold values from -0.125 to 0.125
Outputs:
- mixer_result: bfloat16 [16384, 4096], P(('ep', 'tp'))
- routed_result: bfloat16 [16384, 4096], P(('ep', 'tp'))
Inputs may be any that keep to these rules, and one draw needn't show every extreme that they name: `expert_ids`: the two numbers of a row differ. In each aligned block of 128 rows no expert is named by more than 10 rows, and in every draw some expert is named by exactly 10 rows of some block.
All inputs are finite; a program needn't handle non-finite values.
Results may differ from a plain program's by a relative error of at most 0.011.
Values may be sent and summed in bfloat16 or wider, within the bound.
No kernel may reach another device: no remote copies, remote signals or barrier semaphores. Data moves between devices by JAX's collectives and lax.ppermute only.
A program may use at most 192 MiB of HBM per device.

v0:
```python
import functools

import jax
import jax.numpy as jnp
from jax import lax
from jax.experimental import pallas as pl
from jax.experimental.pallas import tpu as pltpu
from jax.sharding import PartitionSpec as P


RETURN_PIECES = 2
f32 = jnp.float32
bf16 = jnp.bfloat16
i32 = jnp.int32


def turned(value, axis, steps):
    count = lax.axis_size(axis)
    return lax.ppermute(value, axis, [(i, (i + steps) % count) for i in range(count)])


def dot(a, b):
    return jnp.dot(a, b, preferred_element_type=f32)


def call(body, grid, ins, outs, scratch=(), flops=0, moved=0, prefetch=1):
    return pl.pallas_call(
        body,
        out_shape=[jax.ShapeDtypeStruct(shape, kind) for shape, kind, _ in outs],
        grid_spec=pltpu.PrefetchScalarGridSpec(
            num_scalar_prefetch=prefetch,
            grid=grid,
            in_specs=ins,
            out_specs=[spec for _, _, spec in outs],
            scratch_shapes=list(scratch),
        ),
        cost_estimate=pl.CostEstimate(flops=flops, bytes_accessed=moved, transcendentals=0),
    )


def whole(shape):
    return pl.BlockSpec(shape, lambda *_: (0,) * len(shape), pipeline_mode=pl.Buffered(1))


def one_hot_rows(code_ref, slots, rows, tile=0):
    slot = lax.broadcasted_iota(i32, (slots, rows), 0) + tile * slots
    picks = (slot == code_ref[0:1, :]) | (slot == code_ref[1:2, :])
    return jnp.where(picks, 1.0, 0.0).astype(bf16)


def near_body(q_ref, code_ref, x_ref, gain_ref, out_ref, factor_ref, normed_ref, *, quarter, half):
    step = pl.program_id(0)
    block, width = x_ref.shape
    side = out_ref.shape[1]

    @pl.when(step < half)
    def _():
        x = x_ref[...].astype(f32)
        factor = lax.rsqrt(jnp.sum(x * x, axis=1, keepdims=True) / width + 1e-06)
        factor_ref[...] = jnp.broadcast_to(factor, factor_ref.shape)
        columns = pl.ds(pl.multiple_of(q_ref[0] * quarter, quarter), side)
        piece = x_ref[:, columns].astype(f32) * factor * gain_ref[:, columns].astype(f32)
        normed_ref[pl.ds(step * block, block), :] = piece.astype(bf16)

    @pl.when(step >= half)
    def _():
        picks = one_hot_rows(code_ref, out_ref.shape[0], normed_ref.shape[0], step - half)
        out_ref[...] = dot(picks, normed_ref[...]).astype(bf16)


def near_rows(index, code, x, gain, slots, side):
    rows, width = x.shape
    quarter = width // 4
    half = 4
    block, tile = rows // half, slots // half
    return call(
        functools.partial(near_body, quarter=quarter, half=half),
        (2 * half,),
        [
            whole(code.shape),
            pl.BlockSpec((block, width), lambda i, q: (jnp.minimum(i, half - 1), 0)),
            whole(gain.shape),
        ],
        [
            (
                (slots, side),
                bf16,
                pl.BlockSpec((tile, side), lambda i, q: (jnp.maximum(i - half, 0), 0)),
            ),
            (
                (rows, 128),
                f32,
                pl.BlockSpec((block, 128), lambda i, q: (jnp.minimum(i, half - 1), 0)),
            ),
        ],
        [pltpu.VMEM((rows, side), bf16)],
        2 * slots * rows * side,
        2 * (rows * width + slots * side),
    )(index, code, x, gain)


def far_body(q_ref, code_ref, x0, x1, x2, x3, g0, g1, g2, g3, factor_ref, out_ref, normed_ref):
    @pl.when(pl.program_id(0) == 0)
    def _():
        at = 0
        for x_ref, gain_ref in ((x0, g0), (x1, g1), (x2, g2), (x3, g3)):
            size = x_ref.shape[1]
            piece = x_ref[...].astype(f32) * factor_ref[:, 0:1] * gain_ref[...].astype(f32)
            normed_ref[:, at : at + size] = piece.astype(bf16)
            at += size

    picks = one_hot_rows(code_ref, out_ref.shape[0], normed_ref.shape[0], pl.program_id(0))
    out_ref[...] = dot(picks, normed_ref[...]).astype(bf16)


def far_rows(index, code, x, gain, factor, slots, side):
    rows, width = x.shape
    quarter = width // 4
    rest = quarter - side
    each = quarter // rest
    total = quarter + 3 * rest
    steps = 4

    def last(step):
        return (rest, lambda i, q: (0, (q[0] + step) % 4 * each + each - 1))

    places = [(quarter, lambda i, q: (0, (q[0] + 2) % 4)), last(0), last(1), last(3)]
    once = pl.Buffered(1)
    return call(
        far_body,
        (steps,),
        [whole(code.shape)]
        + [pl.BlockSpec((rows, size), place, pipeline_mode=once) for size, place in places]
        + [pl.BlockSpec((1, size), place, pipeline_mode=once) for size, place in places]
        + [whole(factor.shape)],
        [((slots, total), bf16, pl.BlockSpec((slots // steps, total), lambda i, q: (i, 0)))],
        [pltpu.VMEM((rows, total), bf16)],
        2 * slots * rows * total,
        2 * (rows + slots) * total,
    )(index, code, x, x, x, x, gain, gain, gain, gain, factor)[0]


def first_body(q_ref, x_ref, wg_ref, wu_ref, gate_ref, up_ref):
    gate_ref[...] = dot(x_ref[...], wg_ref[...])
    up_ref[...] = dot(x_ref[...], wu_ref[...])


def first_part(index, x, wg, wu):
    slots, side = x.shape
    units = wg.shape[1]
    quarter = wg.shape[0] // 4
    tile = slots // 4
    weight = pl.BlockSpec(
        (pl.Element(side), pl.Element(units)),
        lambda i, q: (q[0] * quarter, 0),
        pipeline_mode=pl.Buffered(1),
    )
    rowed = pl.BlockSpec((tile, units), lambda i, q: (i, 0))
    return call(
        first_body,
        (4,),
        [pl.BlockSpec((tile, side), lambda i, q: (i, 0)), weight, weight],
        [((slots, units), f32, rowed), ((slots, units), f32, rowed)],
        (),
        4 * slots * side * units,
        2 * slots * side + 4 * side * units + 8 * slots * units,
    )(index, x, wg, wu)


def hidden_body(q_ref, far_ref, right_ref, left_ref, gate_ref, up_ref, *refs, capacity):
    weights, out_ref = refs[:-1], refs[-1]
    many = len(weights) // 2
    parts, count, units = out_ref.shape
    size = parts * count

    def total(start_ref, own):
        value = start_ref[...] + dot(right_ref[...], own[0][...]) + dot(left_ref[...], own[1][...])
        at = 0
        for weight_ref in own[2:]:
            rows = weight_ref.shape[0]
            value += dot(far_ref[:, at : at + rows], weight_ref[...])
            at += rows
        return value

    gate = total(gate_ref, weights[:many])
    up = total(up_ref, weights[many:])
    hidden = (gate / (1.0 + jnp.exp(-gate)) * up).astype(bf16)
    row = lax.broadcasted_iota(i32, (size, 1), 0)
    place = row % count // capacity * (parts * capacity) + row // count * capacity + row % capacity
    column = lax.broadcasted_iota(i32, (size, size), 1)
    order = jnp.where(column == place, 1.0, 0.0).astype(bf16)
    out_ref[...] = dot(order, hidden).astype(bf16).reshape(parts, count, units)


def hidden_units(index, far, right, left, gate, up, wg, wu, capacity):
    slots, side = right.shape
    units = wg.shape[1]
    quarter = wg.shape[0] // 4
    rest = quarter - side
    each = quarter // rest
    steps, parts = 4, 4
    tile = slots // steps
    once = pl.Buffered(1)

    def lent(step):
        return pl.BlockSpec(
            (pl.Element(side), pl.Element(units)),
            lambda i, q: ((q[0] + step) % 4 * quarter, 0),
            pipeline_mode=once,
        )

    def last(step):
        return pl.BlockSpec(
            (rest, units),
            lambda i, q: ((q[0] + step) % 4 * each + each - 1, 0),
            pipeline_mode=once,
        )

    weights = [
        lent(1),
        lent(3),
        pl.BlockSpec((quarter, units), lambda i, q: ((q[0] + 2) % 4, 0), pipeline_mode=once),
        last(0),
        last(1),
        last(3),
    ]
    depth = far.shape[1] + 2 * side

    def rowed(size):
        return pl.BlockSpec((tile, size), lambda i, q: (i, 0))

    return call(
        functools.partial(hidden_body, capacity=capacity),
        (steps,),
        [rowed(far.shape[1]), rowed(side), rowed(side), rowed(units), rowed(units)] + weights * 2,
        [
            (
                (parts, slots // parts, units),
                bf16,
                pl.BlockSpec((parts, tile // parts, units), lambda i, q: (0, i, 0)),
            )
        ],
        (),
        4 * slots * depth * units,
        2 * slots * depth + 4 * depth * units + 10 * slots * units,
    )(index, far, right, left, gate, up, *[wg] * 6, *[wu] * 6)[0]


def rows_of(hidden, step):
    parts, count, units = hidden.shape
    return pl.BlockSpec(
        (None, count, units), lambda i, q: ((q[0] + step) % parts, 0, 0), pipeline_mode=pl.Buffered(1)
    )


def sides_body(q_ref, to_right_ref, to_left_ref, down_ref, right_ref, left_ref):
    right_ref[...] = dot(to_right_ref[...], down_ref[...]).astype(bf16)
    left_ref[...] = dot(to_left_ref[...], down_ref[...]).astype(bf16)


def side_rows(index, hidden, down, piece, pieces):
    _, count, units = hidden.shape
    width = down.shape[1] // pieces
    steps = 4
    tile = width // steps
    tiled = pl.BlockSpec((count, tile), lambda i, q: (0, i))
    return call(
        sides_body,
        (steps,),
        [
            rows_of(hidden, 1),
            rows_of(hidden, 3),
            pl.BlockSpec((units, tile), lambda i, q: (0, piece * steps + i)),
        ],
        [((count, width), bf16, tiled), ((count, width), bf16, tiled)],
        (),
        4 * count * units * width,
        2 * (2 * count * units + units * width + 2 * count * width),
    )(index, hidden, hidden, down)


def own_body(q_ref, rows_ref, down_ref, out_ref):
    out_ref[...] = dot(rows_ref[...], down_ref[...]).astype(bf16)


def own_rows(index, hidden, down, piece, pieces):
    _, count, units = hidden.shape
    width = down.shape[1] // pieces
    steps = 4
    tile = width // steps
    return call(
        own_body,
        (steps,),
        [
            rows_of(hidden, 0),
            pl.BlockSpec((units, tile), lambda i, q: (0, piece * steps + i)),
        ],
        [((count, width), bf16, pl.BlockSpec((count, tile), lambda i, q: (0, i)))],
        (),
        2 * count * units * width,
        2 * (count * units + units * width + count * width),
    )(index, hidden, down)[0]


def messages_of(value, fold, capacity, parts):
    many = value.shape[0]
    size, each = many * parts, parts * capacity
    row = lax.broadcasted_iota(i32, (size, 1), 0)
    place = row % each // capacity * many + row // each * capacity + row % capacity
    column = lax.broadcasted_iota(i32, (size, size), 1)
    order = jnp.where(column == place, 1.0, 0.0).astype(bf16)
    stack = jnp.concatenate([value[:, k * fold : (k + 1) * fold] for k in range(parts)], axis=0)
    return dot(order, stack).astype(bf16)


def across_body(q_ref, rows_ref, down_ref, out_ref, value_ref, *, capacity, parts, steps):
    step = pl.program_id(0)
    tile, fold, many = down_ref.shape[1], out_ref.shape[1], out_ref.shape[0] // parts

    @pl.when(step < steps)
    def _():
        columns = pl.ds(pl.multiple_of(step * tile, tile), tile)
        value_ref[:, columns] = dot(rows_ref[...], down_ref[...]).astype(bf16)

    @pl.when(step >= steps)
    def _():
        value = value_ref[pl.ds(pl.multiple_of((step - steps) * many, many), many), :]
        out_ref[...] = messages_of(value, fold, capacity, parts)


def across_messages(index, hidden, down, piece, pieces, capacity):
    parts, count, units = hidden.shape
    width = down.shape[1] // pieces
    slots, fold = parts * count, width // parts
    steps = 4
    tile = width // steps
    return call(
        functools.partial(across_body, capacity=capacity, parts=parts, steps=steps),
        (2 * steps,),
        [
            rows_of(hidden, 2),
            pl.BlockSpec(
                (units, tile), lambda i, q: (0, piece * steps + jnp.minimum(i, steps - 1))
            ),
        ],
        [
            (
                (slots, fold),
                bf16,
                pl.BlockSpec((slots // steps, fold), lambda i, q: (jnp.maximum(i - steps, 0), 0)),
            )
        ],
        [pltpu.VMEM((count, width), bf16)],
        2 * count * units * width,
        2 * (count * units + units * width + count * width),
    )(index, hidden, down)[0]


def summed_body(q_ref, own_ref, left_ref, right_ref, out_ref, *, capacity, parts):
    total = own_ref[...].astype(f32) + left_ref[...].astype(f32) + right_ref[...].astype(f32)
    out_ref[...] = messages_of(total.astype(bf16), out_ref.shape[1], capacity, parts)


def summed_messages(index, own, left, right, capacity, parts):
    count, width = own.shape
    slots, fold = count * parts, width // parts
    steps = 4
    rowed = pl.BlockSpec((count // steps, width), lambda i, q: (i, 0))
    return call(
        functools.partial(summed_body, capacity=capacity, parts=parts),
        (steps,),
        [rowed, rowed, rowed],
        [((slots, fold), bf16, pl.BlockSpec((slots // steps, fold), lambda i, q: (i, 0)))],
        (),
        2 * slots * slots // 4 * fold,
        8 * count * width,
    )(index, own, left, right)[0]


def combine_body(q_ref, home_ref, share_ref, rows_ref, *refs, capacity, parts):
    out_ref, weight_ref, value_ref = refs[-3:]
    extra = refs[0] if len(refs) > 3 else None
    step = pl.program_id(0)
    slots, tile = rows_ref.shape
    block, width = out_ref.shape

    @pl.when(step == 0)
    def _():
        column = lax.broadcasted_iota(i32, (block, slots), 1)
        for k in range(parts):
            home = home_ref[...] + k * capacity
            weights = jnp.where(column == home[:, 0:1], share_ref[:, 0:1], 0.0)
            weights = jnp.where(column == home[:, 1:2], share_ref[:, 1:2], weights)
            weight_ref[k * block : (k + 1) * block, :] = weights.astype(bf16)

    value_ref[...] = dot(weight_ref[...], rows_ref[...])
    for k in range(parts):
        columns = pl.ds(pl.multiple_of(k * (width // parts) + step * tile, tile), tile)
        value = value_ref[k * block : (k + 1) * block, :]
        if extra is not None:
            value = value + extra[:, columns].astype(f32)
        out_ref[:, columns] = value.astype(bf16)


def combined(index, home, share, rows, capacity, parts, extra=None, into=None, piece=0, pieces=1):
    slots, fold = rows.shape
    block = home.shape[0]
    width = parts * fold
    steps = 2
    placed = pl.BlockSpec((block, width), lambda i, q: (0, piece), pipeline_mode=pl.Buffered(1))
    ins = [
        whole(home.shape),
        whole(share.shape),
        pl.BlockSpec((slots, fold // steps), lambda i, q: (0, i)),
    ]
    args = [home, share, rows]
    if extra is not None:
        ins.append(placed)
        args.append(extra)
    if into is not None:
        ins.append(pl.BlockSpec(memory_space=pl.ANY))
        args.append(into)
    return pl.pallas_call(
        functools.partial(combine_body, capacity=capacity, parts=parts),
        out_shape=jax.ShapeDtypeStruct((block, width * pieces), bf16),
        grid_spec=pltpu.PrefetchScalarGridSpec(
            num_scalar_prefetch=1,
            grid=(steps,),
            in_specs=ins,
            out_specs=placed,
            scratch_shapes=[
                pltpu.VMEM((parts * block, slots), bf16),
                pltpu.VMEM((parts * block, fold // steps), f32),
            ],
        ),
        input_output_aliases={} if into is None else {len(args): 0},
        cost_estimate=pl.CostEstimate(
            flops=2 * parts * block * slots * fold,
            bytes_accessed=2 * slots * fold + 4 * block * width,
            transcendentals=0,
        ),
        name="combined",
    )(index, *args)


def mixed_body(q_ref, hidden_ref, weight_ref, own_ref, *outs):
    step = pl.program_id(0)
    parts = 4
    block = own_ref.shape[0]
    middle = pl.num_programs(0) // 2

    def rows_for(which):
        start = pl.multiple_of((q_ref[0] + which) % parts * block, block)
        return dot(hidden_ref[pl.ds(start, block), :], weight_ref[...]).astype(bf16)

    own_ref[...] = rows_for(0)

    @pl.when(step < middle)
    def _():
        for k in range(parts - 1):
            outs[2 * k][...] = rows_for(k + 1)

    @pl.when(step >= middle)
    def _():
        for k in range(parts - 1):
            outs[2 * k + 1][...] = rows_for(k + 1)


def mixed_rows(index, hidden, weight, parts):
    rows, channels = hidden.shape
    width = weight.shape[1]
    steps = 4
    block, tile = rows // parts, width // steps
    low = pl.BlockSpec((block, tile), lambda i, q: (0, jnp.minimum(i, steps // 2 - 1)))
    high = pl.BlockSpec((block, tile), lambda i, q: (0, jnp.maximum(i - steps // 2, 0)))
    return call(
        mixed_body,
        (steps,),
        [whole(hidden.shape), pl.BlockSpec((channels, tile), lambda i, q: (0, i))],
        [((block, width), bf16, pl.BlockSpec((block, tile), lambda i, q: (0, i)))]
        + [((block, width // 2), bf16, low), ((block, width // 2), bf16, high)] * (parts - 1),
        (),
        2 * rows * channels * width,
        2 * (rows * channels + channels * width + rows * width),
    )(index, hidden, weight)


def on_device(
    mixer_value,
    mixer_gate,
    mixer_taps,
    mixer_gain,
    mixer_weight,
    routed_input,
    routed_gain,
    expert_ids,
    route_share,
    gate_weight,
    up_weight,
    down_weight,
):
    parts = lax.axis_size("tp")
    sources = lax.axis_size("ep")
    q = lax.axis_index("tp").astype(i32)
    index = q.reshape(1)
    across = (q + 2) % parts
    rows, width = routed_input.shape
    block = rows // parts
    chosen = expert_ids.shape[1]
    capacity = 5 * block // (2 * sources)
    per_source = parts * capacity
    slots = sources * per_source
    quarter = width // parts
    side = 7 * quarter // 8

    ids = expert_ids.T.reshape(chosen, parts, block)
    earlier = jnp.arange(block)[:, None] < jnp.arange(block)[None, :]
    same = ids[:, None, :, :, None] == ids[None, :, :, None, :]
    rank = jnp.sum((same & earlier).astype(i32), axis=(0, 3))
    code = ids * per_source + jnp.arange(parts, dtype=i32)[None, :, None] * capacity + rank
    code = code.reshape(chosen, rows)

    def exchanged(messages):
        size = messages.shape[1]
        messages = messages.reshape(sources, per_source, size)
        return lax.all_to_all(messages, "ep", 0, 0, tiled=True).reshape(slots, size)

    taps = mixer_taps.shape[0]
    length = mixer_value.shape[0]
    gated = (mixer_value.astype(f32) * jax.nn.sigmoid(mixer_gate.astype(f32))).astype(bf16)
    before = lax.ppermute(
        gated[length - (taps - 1) :], "ep", [(i, i + 1) for i in range(sources - 1)]
    )

    gain = routed_gain.reshape(1, width)
    near, factor = near_rows(index, code, routed_input, gain, slots, side)
    near, before = lax.optimization_barrier((near, before))
    near = exchanged(near)

    extended = jnp.concatenate([before, gated], axis=0).astype(f32)
    taps_float = mixer_taps.astype(f32)
    filtered = taps_float[0] * extended[0:length]
    for offset in range(1, taps):
        filtered = filtered + taps_float[offset] * extended[offset : offset + length]
    stats = jnp.stack([jnp.sum(filtered, axis=1), jnp.sum(filtered * filtered, axis=1)])
    stats = stats + turned(stats, "tp", 1) + turned(stats, "tp", -1) + turned(stats, "tp", 2)
    channels = mixer_taps.shape[1] * parts
    center = stats[0] / channels
    spread = stats[1] / channels - center * center
    normed_mix = (
        (filtered - center[:, None])
        * lax.rsqrt(spread + 1e-05)[:, None]
        * mixer_gain.astype(f32)
    )
    mixer_hidden = jax.nn.silu(normed_mix).astype(bf16)
    mix_own, right_low, right_high, far_low, far_high, left_low, left_high = mixed_rows(
        index, mixer_hidden, mixer_weight, parts
    )
    via_right, via_left = turned(far_low, "tp", 1), turned(far_high, "tp", -1)
    raw_high, raw_low = turned(right_high, "tp", 1), turned(left_low, "tp", -1)

    factor, right_low, left_high = lax.optimization_barrier((factor, right_low, left_high))
    far = far_rows(index, code, routed_input, gain, factor, slots, side)
    from_left, from_right = turned(near, "tp", 1), turned(near, "tp", -1)
    far = exchanged(far)

    gate, up = first_part(index, near, gate_weight[0], up_weight[0])
    hidden = hidden_units(
        index, far, from_right, from_left, gate, up, gate_weight[0], up_weight[0], capacity
    )

    hidden, right_low, left_high = lax.optimization_barrier((hidden, right_low, left_high))
    sum_low = turned((right_low.astype(f32) + via_right.astype(f32)).astype(bf16), "tp", 1)
    sum_high = turned((left_high.astype(f32) + via_left.astype(f32)).astype(bf16), "tp", -1)
    middle = width // 2
    mixer_result = jnp.concatenate(
        [
            mix_own[:, :middle].astype(f32) + sum_low.astype(f32) + raw_low.astype(f32),
            mix_own[:, middle:].astype(f32) + sum_high.astype(f32) + raw_high.astype(f32),
        ],
        axis=1,
    ).astype(bf16)

    def home_of(which):
        own_ids = lax.dynamic_slice_in_dim(ids, which, 1, 1)[:, 0]
        own_rank = lax.dynamic_slice_in_dim(rank, which, 1, 1)[:, 0]
        own_share = lax.dynamic_slice_in_dim(route_share, which * block, block, 0)
        return (own_ids * per_source + own_rank).T, own_share

    down = down_weight[0]
    far_home, own_home = home_of(across), home_of(q)
    pieces = RETURN_PIECES
    got = []
    for piece in range(pieces):
        to_right, to_left = side_rows(index, hidden, down, piece, pieces)
        got.append((turned(to_right, "tp", 1), turned(to_left, "tp", -1)))
    messages = across_messages(index, hidden, down, 0, 1, capacity)
    far_back = exchanged(messages)
    extra = combined(index, *far_home, far_back, capacity, parts)
    own = [own_rows(index, hidden, down, piece, pieces) for piece in range(pieces)]
    extra, own[-1] = lax.optimization_barrier((extra, own[-1]))
    extra = turned(extra, "tp", 2)
    result = None
    for piece in range(pieces):
        messages = summed_messages(index, own[piece], *got[piece], capacity, parts)
        back = exchanged(messages)
        result = combined(
            index, *own_home, back, capacity, parts, extra, result, piece, pieces
        )
    return (mixer_result, result)


def solution(mesh):
    return jax.shard_map(
        on_device,
        mesh=mesh,
        in_specs=(
            P("ep", "tp"),
            P("ep", "tp"),
            P(None, "tp"),
            P("tp"),
            P("tp", None),
            P("ep", None),
            P(),
            P("ep", None),
            P("ep", None),
            P("ep", None, "tp"),
            P("ep", None, "tp"),
            P("ep", "tp", None),
        ),
        out_specs=(P(("ep", "tp"), None), P(("ep", "tp"), None)),
        check_vma=False,
    )
```

profile of v0, /device:TPU:0, one launch (start us, length us, event | category | flops | bytes accessed | tf_op | source)
XLA Modules:
  0.0 288.0 jit_solution(3217929973160175449)
XLA Ops:
  0.7 1.5 multiply_convert_fusion.1
  2.2 1.3 collective-permute-start
  3.7 0.6 reshape.92.gain_ref.g0.g1.g2.g3
  4.6 0.2 convert_reduce_fusion
  4.8 0.6 bitcast_add_fusion.code_ref
  5.4 7.1 %shard_map.131 = (bf16[1280,896]{1,0:T(8,128)(2,1)}, f32[512,128]{1,0:T(8,128)}) custom-call(s32[1]{0:T(128)} %bitcast.q_ref, s32[2,512]{1,0:T(2,128)} %bitcast_add_fusion.code_ref, bf16[512,4096]{1,0:T(8,128)(2,1)} %x3.1, bf16[1,4096]{1,0:T(2,128)(2,1)} %reshape.92.gain_ref.g0.g1.g2.g3), custom_call_target="tpu_custom_call" | custom-call | flops 1174405120 | bytes 6488064 | tf_op jit(solution)/shard_map/pallas_call | solution.py:76
  12.5 10.1 %all-to-all-start.1 = ((bf16[32,40,896]{2,1,0:T(8,128)(2,1)}), bf16[32,40,896]{2,1,0:T(8,128)(2,1)S(1)}, u32[]{:S(2)}, u32[]{:S(2)}) async-start(bf16[32,40,896]{2,1,0:T(8,128)(2,1)} %bitcast.94), calls=%async_computation.1 | async-start | bytes 4587520 | tf_op jit(solution)/shard_map/all_to_all | solution.py:526
  22.6 0.2 maximum_convert_fusion
  22.8 5.0 %fusion.30 = (f32[512]{0:T(512)S(1)}, f32[512]{0:T(512)S(1)}, f32[512,512]{1,0:T(8,128)S(1)}) fusion(f32[542,512]{1,0:T(8,128)S(1)} %maximum_convert_fusion, f32[512]{0:T(512)S(1)} %bitcast.116, f32[512]{0:T(512)S(1)} %bitcast.115, f32[512]{0:T(512)S(1)} %bitcast.114, f32[512]{0:T(512)S(1)} %bitcast.113, f32[512]{0:T(512)S(1)} %bitcast.112, ...), kind=kLoop, calls=%fused_computation.86 | loop fusion | flops 16776192 | bytes 33622016 | tf_op jit(solution)/shard_map/reduce_sum | solution.py:545
  27.8 2.8 collective-permute-start.2
  30.6 0.8 collective-permute-start.3
  31.5 0.9 collective-permute-start.1
  32.3 3.4 %collective-permute-done.3 = f32[2,512]{1,0:T(2,128)S(1)} collective-permute-done((f32[2,512]{1,0:T(2,128)S(1)}, f32[2,512]{1,0:T(2,128)S(1)}, u32[]{:S(2)}, u32[]{:S(2)}) %collective-permute-start.3) | collective-permute-done | bytes 4128 | tf_op jit(solution)/shard_map/ppermute | solution.py:19
  35.8 0.5 collective-permute-done.1
  36.3 1.2 multiply_convert_fusion.hidden_ref
  37.5 7.0 %shard_map.132 = (bf16[128,4096]{1,0:T(8,128)(2,1)}, bf16[128,2048]{1,0:T(8,128)(2,1)}, bf16[128,2048]{1,0:T(8,128)(2,1)}, bf16[128,2048]{1,0:T(8,128)(2,1)}, bf...) custom-call(s32[1]{0:T(128)} %bitcast.q_ref, ...), custom_call_target="tpu_custom_call" | custom-call | flops 2147483648 | bytes 8912896 | tf_op jit(solution)/shard_map/pallas_call | solution.py:476
  44.5 6.0 %shard_map.133 = bf16[1280,1408]{1,0:T(8,128)(2,1)} custom-call(s32[1]{0:T(128)} %bitcast.q_ref, s32[2,512]{1,0:T(2,128)} %bitcast_add_fusion.code_ref, bf16[512,4096]{1,0:T(8,128)(2,1)} %x3.1, bf16[512,4096]{1,0:T(8,128)(2,1)} %x3.1, bf16[512,4096]{1,0:T(8,128)(2,1)} %x3.1, bf16[512,4096]{1,0:T(8,128)(2,1)} %x3.1, ...), custom_call_target="tpu_custom_call" | custom-call | flops 1845493760 | bytes 5046272 | tf_op jit(solution)/shard_map/pallas_call | solution.py:129
  50.5 4.4 %all-to-all-done.1 = bf16[32,40,896]{2,1,0:T(8,128)(2,1)S(1)} async-done(((bf16[32,40,896]{2,1,0:T(8,128)(2,1)}), bf16[32,40,896]{2,1,0:T(8,128)(2,1)S(1)}, u32[]{:S(2)}, u32[]{:S(2)}) %all-to-all-start.1) | async-done | bytes 2293792 | tf_op jit(solution)/shard_map/all_to_all | solution.py:526
  54.9 4.8 %all-to-all-start = ((bf16[32,40,1408]{2,1,0:T(8,128)(2,1)}), bf16[32,40,1408]{2,1,0:T(8,128)(2,1)}, u32[]{:S(2)}, u32[]{:S(2)}) async-start(bf16[32,40,1408]{2,1,0:T(8,128)(2,1)} %bitcast.84), calls=%async_computation | async-start | bytes 7208960 | tf_op jit(solution)/shard_map/all_to_all | solution.py:526
  59.8 1.6 collective-permute-start.5
  61.3 1.7 collective-permute-start.4
  63.1 6.4 %shard_map.134 = (f32[1280,512]{1,0:T(8,128)}, f32[1280,512]{1,0:T(8,128)}) custom-call(s32[1]{0:T(128)} %bitcast.q_ref, bf16[1280,896]{1,0:T(8,128)(2,1)} %bitcast.88, bf16[4096,512]{1,0:T(8,128)(2,1)} %bitcast.65, bf16[4096,512]{1,0:T(8,128)(2,1)} %bitcast.72), custom_call_target="tpu_custom_call" | custom-call | flops 2348810240 | bytes 9371648 | tf_op jit(solution)/shard_map/pallas_call | solution.py:159
  69.5 37.5 %all-to-all-done = bf16[32,40,1408]{2,1,0:T(8,128)(2,1)} async-done(((bf16[32,40,1408]{2,1,0:T(8,128)(2,1)}), bf16[32,40,1408]{2,1,0:T(8,128)(2,1)}, u32[]{:S(2)}, u32[]{:S(2)}) %all-to-all-start) | async-done | bytes 3604512 | tf_op jit(solution)/shard_map/all_to_all | solution.py:526
  106.9 6.1 %collective-permute-done.5.left_ref = bf16[1280,896]{1,0:T(8,128)(2,1)} collective-permute-done((bf16[1280,896]{1,0:T(8,128)(2,1)S(1)}, bf16[1280,896]{1,0:T(8,128)(2,1)}, u32[]{:S(2)}, u32[]{:S(2)}) %collective-permute-start.5) | collective-permute-done | bytes 2293792 | tf_op jit(solution)/shard_map/ppermute | solution.py:19
  113.0 17.7 %shard_map.135.rows_ref.to_right_ref.to_left_ref = bf16[4,320,512]{2,1,0:T(8,128)(2,1)} custom-call(s32[1]{0:T(128)} %bitcast.q_ref, bf16[1280,1408]{1,0:T(8,128)(2,1)} %bitcast.40.far_ref, bf16[1280,896]{1,0:T(8,128)(2,1)} %collective-permute-done.4.right_ref, bf16[1280,896]{1,0:T(8,128)(2,1)} %collective-permute-done.5.left_ref, ...), custom_call_target="tpu_custom_call" | custom-call | flops 8388608000 | bytes 21299200 | tf_op jit(solution)/shard_map/pallas_call | solution.py:232
  130.7 8.1 %shard_map.136 = bf16[1280,1024]{1,0:T(8,128)(2,1)} custom-call(s32[1]{0:T(128)} %bitcast.q_ref, bf16[4,320,512]{2,1,0:T(8,128)(2,1)} %shard_map.135.rows_ref.to_right_ref.to_left_ref, bf16[512,4096]{1,0:T(8,128)(2,1)} %bitcast.79), custom_call_target="tpu_custom_call" | custom-call | flops 1342177280 | bytes 7143424 | tf_op jit(solution)/shard_map/pallas_call | solution.py:337
  138.8 7.3 %all-to-all-start.2 = ((bf16[32,40,1024]{2,1,0:T(8,128)(2,1)}), bf16[32,40,1024]{2,1,0:T(8,128)(2,1)S(1)}, u32[]{:S(2)}, u32[]{:S(2)}) async-start(bf16[32,40,1024]{2,1,0:T(8,128)(2,1)} %bitcast.85), calls=%async_computation.2 | async-start | bytes 5242880 | tf_op jit(solution)/shard_map/all_to_all | solution.py:526
  146.1 4.9 %shard_map.141 = (bf16[320,2048]{1,0:T(8,128)(2,1)}, bf16[320,2048]{1,0:T(8,128)(2,1)}) custom-call(s32[1]{0:T(128)} %bitcast.q_ref, bf16[4,320,512]{2,1,0:T(8,128)(2,1)} %shard_map.135.rows_ref.to_right_ref.to_left_ref, bf16[4,320,512]{2,1,0:T(8,128)(2,1)} %shard_map.135.rows_ref.to_right_ref.to_left_ref, bf16[512,4096]{1,0:T(8,128)(2,1)} %bitcast.80), custom_call_target="tpu_custom_call" | custom-call | flops 1342177280 | bytes 5373952 | tf_op jit(solution)/shard_map/pallas_call | solution.py:267
  151.0 1.5 collective-permute-start.15
  152.5 1.8 collective-permute-start.16
  154.3 1.8 collective-permute-start.9
  156.1 4.8 %shard_map.138 = (bf16[320,2048]{1,0:T(8,128)(2,1)}, bf16[320,2048]{1,0:T(8,128)(2,1)}) custom-call(s32[1]{0:T(128)} %bitcast.q_ref, bf16[4,320,512]{2,1,0:T(8,128)(2,1)} %shard_map.135.rows_ref.to_right_ref.to_left_ref, bf16[4,320,512]{2,1,0:T(8,128)(2,1)} %shard_map.135.rows_ref.to_right_ref.to_left_ref, bf16[512,4096]{1,0:T(8,128)(2,1)} %bitcast.81), custom_call_target="tpu_custom_call" | custom-call | flops 1342177280 | bytes 5373952 | tf_op jit(solution)/shard_map/pallas_call | solution.py:267
  160.9 0.2 collective-permute-start.12
  161.4 0.7 add_bitcast_fusion
  162.0 0.3 collective-permute-start.6
  162.3 4.4 %shard_map.140.own_ref = bf16[320,2048]{1,0:T(8,128)(2,1)} custom-call(s32[1]{0:T(128)} %bitcast.q_ref, bf16[4,320,512]{2,1,0:T(8,128)(2,1)} %shard_map.135.rows_ref.to_right_ref.to_left_ref, bf16[512,4096]{1,0:T(8,128)(2,1)} %bitcast.82), custom_call_target="tpu_custom_call" | custom-call | flops 671088640 | bytes 3735552 | tf_op jit(solution)/shard_map/pallas_call | solution.py:291
  166.8 17.5 %collective-permute-done.15.left_ref = bf16[320,2048]{1,0:T(8,128)(2,1)} collective-permute-done((bf16[320,2048]{1,0:T(8,128)(2,1)}, bf16[320,2048]{1,0:T(8,128)(2,1)}, u32[]{:S(2)}, u32[]{:S(2)}) %collective-permute-start.15) | collective-permute-done | bytes 1310752 | tf_op jit(solution)/shard_map/ppermute | solution.py:19
  184.2 1.8 collective-permute-start.8
  186.0 1.4 collective-permute-start.13
  187.5 5.1 %shard_map.142 = bf16[1280,512]{1,0:T(8,128)(2,1)} custom-call(s32[1]{0:T(128)} %bitcast.q_ref, bf16[320,2048]{1,0:T(8,128)(2,1)} %shard_map.140.own_ref, bf16[320,2048]{1,0:T(8,128)(2,1)} %collective-permute-done.15.left_ref, bf16[320,2048]{1,0:T(8,128)(2,1)} %collective-permute-done.16.right_ref), custom_call_target="tpu_custom_call" | custom-call | flops 419430400 | bytes 5242880 | tf_op jit(solution)/shard_map/pallas_call | solution.py:369
  192.5 3.2 %collective-permute-done.9 = bf16[128,2048]{1,0:T(8,128)(2,1)} collective-permute-done((bf16[128,2048]{1,0:T(8,128)(2,1)}, bf16[128,2048]{1,0:T(8,128)(2,1)}, u32[]{:S(2)}, u32[]{:S(2)}) %collective-permute-start.9) | collective-permute-done | bytes 524320 | tf_op jit(solution)/shard_map/ppermute | solution.py:19
  195.7 1.2 collective-permute-start.11
  196.9 1.5 copy-done.4
  198.4 7.4 %all-to-all-start.4 = ((bf16[32,40,512]{2,1,0:T(8,128)(2,1)}), bf16[32,40,512]{2,1,0:T(8,128)(2,1)S(1)}, u32[]{:S(2)}, u32[]{:S(2)}) async-start(bf16[32,40,512]{2,1,0:T(8,128)(2,1)} %bitcast.91), calls=%async_computation.4 | async-start | bytes 2621440 | tf_op jit(solution)/shard_map/all_to_all | solution.py:526
  205.8 2.0 add_convert_fusion.1
  207.8 15.7 %collective-permute-done.6 = bf16[128,2048]{1,0:T(8,128)(2,1)} collective-permute-done((bf16[128,2048]{1,0:T(8,128)(2,1)}, bf16[128,2048]{1,0:T(8,128)(2,1)}, u32[]{:S(2)}, u32[]{:S(2)}) %collective-permute-start.6) | collective-permute-done | bytes 524320 | tf_op jit(solution)/shard_map/ppermute | solution.py:19
  223.5 1.8 collective-permute-start.10
  225.3 1.2 add_convert_fusion.3
  226.5 0.5 collective-permute-start.7
  227.0 0.7 copy.31.share_ref
  227.8 4.4 %shard_map.137.own_ref = bf16[320,2048]{1,0:T(8,128)(2,1)} custom-call(s32[1]{0:T(128)} %bitcast.q_ref, bf16[4,320,512]{2,1,0:T(8,128)(2,1)} %shard_map.135.rows_ref.to_right_ref.to_left_ref, bf16[512,4096]{1,0:T(8,128)(2,1)} %bitcast.83), custom_call_target="tpu_custom_call" | custom-call | flops 671088640 | bytes 3735552 | tf_op jit(solution)/shard_map/pallas_call | solution.py:291
  232.2 4.9 %combined.3 = bf16[128,4096]{1,0:T(8,128)(2,1)} custom-call(s32[1]{0:T(128)} %bitcast.q_ref, s32[128,2]{1,0:T(8,128)} %get-tuple-element.57.home_ref, f32[128,2]{1,0:T(8,128)} %copy.31.share_ref, bf16[1280,1024]{1,0:T(8,128)(2,1)} %bitcast.93), custom_call_target="tpu_custom_call" | custom-call | flops 1342177280 | bytes 4718592 | tf_op jit(solution)/shard_map/combined/pallas_call | solution.py:423
  237.1 5.1 %shard_map.139 = bf16[1280,512]{1,0:T(8,128)(2,1)} custom-call(s32[1]{0:T(128)} %bitcast.q_ref, bf16[320,2048]{1,0:T(8,128)(2,1)} %shard_map.137.own_ref, bf16[320,2048]{1,0:T(8,128)(2,1)} %collective-permute-done.12.left_ref, bf16[320,2048]{1,0:T(8,128)(2,1)} %collective-permute-done.13.right_ref), custom_call_target="tpu_custom_call" | custom-call | flops 419430400 | bytes 5242880 | tf_op jit(solution)/shard_map/pallas_call | solution.py:369
  242.2 1.1 copy-done.2
  243.3 7.4 %all-to-all-start.3 = ((bf16[32,40,512]{2,1,0:T(8,128)(2,1)}), bf16[32,40,512]{2,1,0:T(8,128)(2,1)S(1)}, u32[]{:S(2)}, u32[]{:S(2)}) async-start(bf16[32,40,512]{2,1,0:T(8,128)(2,1)} %bitcast.92), calls=%async_computation.3 | async-start | bytes 2621440 | tf_op jit(solution)/shard_map/all_to_all | solution.py:526
  250.7 1.6 collective-permute-start.14
  252.3 0.7 copy.29.share_ref
  253.0 2.4 add_convert_fusion.2
  255.4 1.0 pad_maximum_fusion
  256.4 21.4 %collective-permute-done.14.refs_0_ = bf16[128,4096]{1,0:T(8,128)(2,1)S(1)} collective-permute-done((bf16[128,4096]{1,0:T(8,128)(2,1)}, bf16[128,4096]{1,0:T(8,128)(2,1)S(1)}, u32[]{:S(2)}, u32[]{:S(2)}) %collective-permute-start.14) | collective-permute-done | bytes 1048608 | tf_op jit(solution)/shard_map/ppermute | solution.py:19
  277.8 1.0 copy-done.3
  278.8 4.0 %combined.4.refs_1_ = bf16[128,4096]{1,0:T(8,128)(2,1)} custom-call(s32[1]{0:T(128)} %bitcast.q_ref, s32[128,2]{1,0:T(8,128)} %get-tuple-element.58.home_ref, f32[128,2]{1,0:T(8,128)} %copy.29.share_ref, bf16[1280,512]{1,0:T(8,128)(2,1)} %bitcast.90, bf16[128,4096]{1,0:T(8,128)(2,1)} %copy-done.3), custom_call_target="tpu_custom_call" | custom-call | flops 671088640 | bytes 2359296 | tf_op jit(solution)/shard_map/combined/pallas_call | solution.py:423
  282.8 1.1 copy-done.1
  283.9 4.0 %combined.5 = bf16[128,4096]{1,0:T(8,128)(2,1)} custom-call(s32[1]{0:T(128)} %bitcast.q_ref, s32[128,2]{1,0:T(8,128)} %get-tuple-element.58.home_ref, f32[128,2]{1,0:T(8,128)} %copy.29.share_ref, bf16[1280,512]{1,0:T(8,128)(2,1)} %bitcast.89, bf16[128,4096]{1,0:T(8,128)(2,1)} %copy-done.3, ...), custom_call_target="tpu_custom_call", output_to_operand_aliasing={{}: (5, {})} | custom-call | flops 671088640 | bytes 2359296 | tf_op jit(solution)/shard_map/combined/pallas_call | solution.py:423
  (50 shorter events, 0.8 us)
Async XLA Ops:
  0.6 2.9 %copy-start.7 = (bf16[31,512]{1,0:T(8,128)(2,1)S(1)}, bf16[31,512]{1,0:T(8,128)(2,1)}, u32[]{:S(2)}) copy-start(bf16[31,512]{1,0:T(8,128)(2,1)} %param.14) | copy-start | bytes 95236
  0.6 3.0 %copy-start.9 = (bf16[4096]{0:T(1024)(128)(2,1)S(1)}, bf16[4096]{0:T(1024)(128)(2,1)}, u32[]{:S(2)}) copy-start(bf16[4096]{0:T(1024)(128)(2,1)} %param.18) | copy-start | bytes 24580
  0.7 3.7 %copy-start.8 = (s32[512,2]{0,1:T(2,128)S(1)}, s32[512,2]{0,1:T(2,128)}, u32[]{:S(2)}) copy-start(s32[512,2]{0,1:T(2,128)} %param.19) | copy-start | bytes 12292
  2.2 10.3 %collective-permute-start = (bf16[30,512]{1,0:T(8,128)(2,1)S(1)}, bf16[30,512]{1,0:T(8,128)(2,1)S(1)}, u32[]{:S(2)}, u32[]{:S(2)}) collective-permute-start(bf16[30,512]{1,0:T(8,128)(2,1)S(1)} %slice.269), channel_id=1, source_target_pairs={{0,4},{4,8},{8,12},{12,16},{16,20},{20,24},{24,28},{28,32},{32,36}... | collective-permute-start | bytes 92168 | tf_op jit(solution)/shard_map/ppermute | solution.py:531
  12.5 42.4 %all-to-all-start.1 = ((bf16[32,40,896]{2,1,0:T(8,128)(2,1)}), bf16[32,40,896]{2,1,0:T(8,128)(2,1)S(1)}, u32[]{:S(2)}, u32[]{:S(2)}) async-start(bf16[32,40,896]{2,1,0:T(8,128)(2,1)} %bitcast.94), calls=%async_computation.1 | async-start | bytes 4587520 | tf_op jit(solution)/shard_map/all_to_all | solution.py:526
  22.7 9.6 %copy-start.10 = (bf16[512]{0:T(512)(128)(2,1)S(1)}, bf16[512]{0:T(512)(128)(2,1)}, u32[]{:S(2)}) copy-start(bf16[512]{0:T(512)(128)(2,1)} %param.15) | copy-start | bytes 3076
  27.8 4.5 %collective-permute-start.2 = (f32[2,512]{1,0:T(2,128)S(1)}, f32[2,512]{1,0:T(2,128)S(1)}, u32[]{:S(2)}, u32[]{:S(2)}) collective-permute-start(f32[2,512]{1,0:T(2,128)S(1)} %pad_maximum_fusion.1), channel_id=1, source_target_pairs={{0,3},{1,0},{2,1},{3,2},{4,7},{5,4},{6,5},{7,6},{8,11},{9,8},{10,9... | collective-permute-start | bytes 12296 | tf_op jit(solution)/shard_map/ppermute | solution.py:19
  30.6 5.1 %collective-permute-start.3 = (f32[2,512]{1,0:T(2,128)S(1)}, f32[2,512]{1,0:T(2,128)S(1)}, u32[]{:S(2)}, u32[]{:S(2)}) collective-permute-start(f32[2,512]{1,0:T(2,128)S(1)} %pad_maximum_fusion.1), channel_id=1, source_target_pairs={{0,2},{1,3},{2,0},{3,1},{4,6},{5,7},{6,4},{7,5},{8,10},{9,11},{10,... | collective-permute-start | bytes 12296 | tf_op jit(solution)/shard_map/ppermute | solution.py:19
  31.5 4.8 %collective-permute-start.1 = (f32[2,512]{1,0:T(2,128)S(1)}, f32[2,512]{1,0:T(2,128)S(1)}, u32[]{:S(2)}, u32[]{:S(2)}) collective-permute-start(f32[2,512]{1,0:T(2,128)S(1)} %pad_maximum_fusion.1), channel_id=1, source_target_pairs={{0,1},{1,2},{2,3},{3,0},{4,5},{5,6},{6,7},{7,4},{8,9},{9,10},{10,1... | collective-permute-start | bytes 12296 | tf_op jit(solution)/shard_map/ppermute | solution.py:19
  54.9 6.4 %copy-start = (bf16[32,40,896]{2,1,0:T(8,128)(2,1)}, bf16[32,40,896]{2,1,0:T(8,128)(2,1)S(1)}, u32[]{:S(2)}) copy-start(bf16[32,40,896]{2,1,0:T(8,128)(2,1)S(1)} %all-to-all-done.1) | copy-start | bytes 6881284
  54.9 52.0 %all-to-all-start = ((bf16[32,40,1408]{2,1,0:T(8,128)(2,1)}), bf16[32,40,1408]{2,1,0:T(8,128)(2,1)}, u32[]{:S(2)}, u32[]{:S(2)}) async-start(bf16[32,40,1408]{2,1,0:T(8,128)(2,1)} %bitcast.84), calls=%async_computation | async-start | bytes 7208960 | tf_op jit(solution)/shard_map/all_to_all | solution.py:526
  59.8 53.2 %collective-permute-start.5 = (bf16[1280,896]{1,0:T(8,128)(2,1)S(1)}, bf16[1280,896]{1,0:T(8,128)(2,1)}, u32[]{:S(2)}, u32[]{:S(2)}) collective-permute-start(bf16[1280,896]{1,0:T(8,128)(2,1)S(1)} %bitcast.86), channel_id=1, source_target_pairs={{0,1},{1,2},{2,3},{3,0},{4,5},{5,6},{6,7},{7,4},{8,9},{9,10},{10,1... | collective-permute-start | bytes 6881288 | tf_op jit(solution)/shard_map/ppermute | solution.py:19
  61.3 51.7 %collective-permute-start.4 = (bf16[1280,896]{1,0:T(8,128)(2,1)S(1)}, bf16[1280,896]{1,0:T(8,128)(2,1)}, u32[]{:S(2)}, u32[]{:S(2)}) collective-permute-start(bf16[1280,896]{1,0:T(8,128)(2,1)S(1)} %bitcast.87), channel_id=1, source_target_pairs={{0,3},{1,0},{2,1},{3,2},{4,7},{5,4},{6,5},{7,6},{8,11},{9,8},{10,9... | collective-permute-start | bytes 6881288 | tf_op jit(solution)/shard_map/ppermute | solution.py:19
  138.8 58.1 %all-to-all-start.2 = ((bf16[32,40,1024]{2,1,0:T(8,128)(2,1)}), bf16[32,40,1024]{2,1,0:T(8,128)(2,1)S(1)}, u32[]{:S(2)}, u32[]{:S(2)}) async-start(bf16[32,40,1024]{2,1,0:T(8,128)(2,1)} %bitcast.85), calls=%async_computation.2 | async-start | bytes 5242880 | tf_op jit(solution)/shard_map/all_to_all | solution.py:526
  151.0 33.2 %collective-permute-start.15 = (bf16[320,2048]{1,0:T(8,128)(2,1)}, bf16[320,2048]{1,0:T(8,128)(2,1)}, u32[]{:S(2)}, u32[]{:S(2)}) collective-permute-start(bf16[320,2048]{1,0:T(8,128)(2,1)} %get-tuple-element.50), channel_id=1, source_target_pairs={{0,1},{1,2},{2,3},{3,0},{4,5},{5,6},{6,7},{7,4},{8,9},{9,10},{10,1... | collective-permute-start | bytes 3932168 | tf_op jit(solution)/shard_map/ppermute | solution.py:19
  152.5 33.5 %collective-permute-start.16 = (bf16[320,2048]{1,0:T(8,128)(2,1)}, bf16[320,2048]{1,0:T(8,128)(2,1)}, u32[]{:S(2)}, u32[]{:S(2)}) collective-permute-start(bf16[320,2048]{1,0:T(8,128)(2,1)} %get-tuple-element.51), channel_id=1, source_target_pairs={{0,3},{1,0},{2,1},{3,2},{4,7},{5,4},{6,5},{7,6},{8,11},{9,8},{10,9... | collective-permute-start | bytes 3932168 | tf_op jit(solution)/shard_map/ppermute | solution.py:19
  154.3 41.4 %collective-permute-start.9 = (bf16[128,2048]{1,0:T(8,128)(2,1)}, bf16[128,2048]{1,0:T(8,128)(2,1)}, u32[]{:S(2)}, u32[]{:S(2)}) collective-permute-start(bf16[128,2048]{1,0:T(8,128)(2,1)} %get-tuple-element.43), channel_id=1, source_target_pairs={{0,3},{1,0},{2,1},{3,2},{4,7},{5,4},{6,5},{7,6},{8,11},{9,8},{10,9... | collective-permute-start | bytes 1572872 | tf_op jit(solution)/shard_map/ppermute | solution.py:19
  160.9 65.6 %collective-permute-start.12 = (bf16[320,2048]{1,0:T(8,128)(2,1)}, bf16[320,2048]{1,0:T(8,128)(2,1)}, u32[]{:S(2)}, u32[]{:S(2)}) collective-permute-start(bf16[320,2048]{1,0:T(8,128)(2,1)} %get-tuple-element.47), channel_id=1, source_target_pairs={{0,1},{1,2},{2,3},{3,0},{4,5},{5,6},{6,7},{7,4},{8,9},{9,10},{10,1... | collective-permute-start | bytes 3932168 | tf_op jit(solution)/shard_map/ppermute | solution.py:19
  162.0 61.5 %collective-permute-start.6 = (bf16[128,2048]{1,0:T(8,128)(2,1)}, bf16[128,2048]{1,0:T(8,128)(2,1)}, u32[]{:S(2)}, u32[]{:S(2)}) collective-permute-start(bf16[128,2048]{1,0:T(8,128)(2,1)} %get-tuple-element.40), channel_id=1, source_target_pairs={{0,1},{1,2},{2,3},{3,0},{4,5},{5,6},{6,7},{7,4},{8,9},{9,10},{10,1... | collective-permute-start | bytes 1572872 | tf_op jit(solution)/shard_map/ppermute | solution.py:19
  184.2 68.8 %collective-permute-start.8 = (bf16[128,2048]{1,0:T(8,128)(2,1)}, bf16[128,2048]{1,0:T(8,128)(2,1)}, u32[]{:S(2)}, u32[]{:S(2)}) collective-permute-start(bf16[128,2048]{1,0:T(8,128)(2,1)} %get-tuple-element.41), channel_id=1, source_target_pairs={{0,3},{1,0},{2,1},{3,2},{4,7},{5,4},{6,5},{7,6},{8,11},{9,8},{10,9... | collective-permute-start | bytes 1572872 | tf_op jit(solution)/shard_map/ppermute | solution.py:19
  186.0 51.1 %collective-permute-start.13 = (bf16[320,2048]{1,0:T(8,128)(2,1)}, bf16[320,2048]{1,0:T(8,128)(2,1)}, u32[]{:S(2)}, u32[]{:S(2)}) collective-permute-start(bf16[320,2048]{1,0:T(8,128)(2,1)} %get-tuple-element.48), channel_id=1, source_target_pairs={{0,3},{1,0},{2,1},{3,2},{4,7},{5,4},{6,5},{7,6},{8,11},{9,8},{10,9... | collective-permute-start | bytes 3932168 | tf_op jit(solution)/shard_map/ppermute | solution.py:19
  195.7 57.3 %collective-permute-start.11 = (bf16[128,2048]{1,0:T(8,128)(2,1)}, bf16[128,2048]{1,0:T(8,128)(2,1)}, u32[]{:S(2)}, u32[]{:S(2)}) collective-permute-start(bf16[128,2048]{1,0:T(8,128)(2,1)} %get-tuple-element.44), channel_id=1, source_target_pairs={{0,1},{1,2},{2,3},{3,0},{4,5},{5,6},{6,7},{7,4},{8,9},{9,10},{10,1... | collective-permute-start | bytes 1572872 | tf_op jit(solution)/shard_map/ppermute | solution.py:19
  196.9 1.5 copy-start.4
  196.9 8.9 %copy-start.6 = (bf16[128,2048]{1,0:T(8,128)(2,1)S(1)}, bf16[128,2048]{1,0:T(8,128)(2,1)}, u32[]{:S(2)}) copy-start(bf16[128,2048]{1,0:T(8,128)(2,1)} %get-tuple-element.42) | copy-start | bytes 1572868
  198.4 43.8 %all-to-all-start.4 = ((bf16[32,40,512]{2,1,0:T(8,128)(2,1)}), bf16[32,40,512]{2,1,0:T(8,128)(2,1)S(1)}, u32[]{:S(2)}, u32[]{:S(2)}) async-start(bf16[32,40,512]{2,1,0:T(8,128)(2,1)} %bitcast.91), calls=%async_computation.4 | async-start | bytes 2621440 | tf_op jit(solution)/shard_map/all_to_all | solution.py:526
  205.8 19.6 %copy-start.5 = (bf16[128,2048]{1,0:T(8,128)(2,1)S(1)}, bf16[128,2048]{1,0:T(8,128)(2,1)}, u32[]{:S(2)}) copy-start(bf16[128,2048]{1,0:T(8,128)(2,1)} %get-tuple-element.39) | copy-start | bytes 1572868
  205.8 21.2 %copy-start.11 = (f32[512,2]{0,1:T(2,128)S(1)}, f32[512,2]{0,1:T(2,128)}, u32[]{:S(2)}) copy-start(f32[512,2]{0,1:T(2,128)} %param.20) | copy-start | bytes 12292
  223.5 29.5 %collective-permute-start.10 = (bf16[128,2048]{1,0:T(8,128)(2,1)}, bf16[128,2048]{1,0:T(8,128)(2,1)}, u32[]{:S(2)}, u32[]{:S(2)}) collective-permute-start(bf16[128,2048]{1,0:T(8,128)(2,1)} %add_convert_fusion.1), channel_id=1, source_target_pairs={{0,3},{1,0},{2,1},{3,2},{4,7},{5,4},{6,5},{7,6},{8,11},{9,8},{10,9... | collective-permute-start | bytes 1572872 | tf_op jit(solution)/shard_map/ppermute | solution.py:19
  226.5 26.5 %collective-permute-start.7 = (bf16[128,2048]{1,0:T(8,128)(2,1)S(1)}, bf16[128,2048]{1,0:T(8,128)(2,1)}, u32[]{:S(2)}, u32[]{:S(2)}) collective-permute-start(bf16[128,2048]{1,0:T(8,128)(2,1)S(1)} %add_convert_fusion.3), channel_id=1, source_target_pairs={{0,1},{1,2},{2,3},{3,0},{4,5},{5,6},{6,7},{7,4},{8,9},{9,10},{10,1... | collective-permute-start | bytes 1572872 | tf_op jit(solution)/shard_map/ppermute | solution.py:19
  242.2 1.1 copy-start.2
  243.3 39.5 %all-to-all-start.3 = ((bf16[32,40,512]{2,1,0:T(8,128)(2,1)}), bf16[32,40,512]{2,1,0:T(8,128)(2,1)S(1)}, u32[]{:S(2)}, u32[]{:S(2)}) async-start(bf16[32,40,512]{2,1,0:T(8,128)(2,1)} %bitcast.92), calls=%async_computation.3 | async-start | bytes 2621440 | tf_op jit(solution)/shard_map/all_to_all | solution.py:526
  250.7 27.1 %collective-permute-start.14 = (bf16[128,4096]{1,0:T(8,128)(2,1)}, bf16[128,4096]{1,0:T(8,128)(2,1)S(1)}, u32[]{:S(2)}, u32[]{:S(2)}) collective-permute-start(bf16[128,4096]{1,0:T(8,128)(2,1)} %combined.3), channel_id=1, source_target_pairs={{0,2},{1,3},{2,0},{3,1},{4,6},{5,7},{6,4},{7,5},{8,10},{9,11},{10,... | collective-permute-start | bytes 3145736 | tf_op jit(solution)/shard_map/ppermute | solution.py:19
  277.8 1.0 copy-start.3
  282.8 1.1 copy-start.1
where the time goes:
time: 290 us; the launch traced here: 288 us
  waiting for transfers between devices  110 us (38%)
  Pallas kernels  94 us (32%)
  starting transfers between devices  60 us (21%)
  other arithmetic  16.1 us (6%)
  local copies, waits for them, and re-layouts  7.38 us (3%)
    ppermute x16, waiting for transfers between devices, turned(): lax.ppermute(value, axis, [(i, (i + steps) % count) for i in range(count)])  67.8 us
    all_to_all x5, waiting for transfers between devices, exchanged(): return lax.all_to_all(messages, 'ep', 0, 0, tiled=True).reshape(slots, size)  41.9 us
    all_to_all x5, starting transfers between devices, exchanged(): return lax.all_to_all(messages, 'ep', 0, 0, tiled=True).reshape(slots, size)  37 us
    ppermute x16, starting transfers between devices, turned(): lax.ppermute(value, axis, [(i, (i + steps) % count) for i in range(count)])  21.7 us
    pallas_call x1, Pallas kernels, hidden_units(): call(functools.partial(hidden_body, capacity=capacity), (steps,), [rowed(...  17.7 us
    pallas_call x3, Pallas kernels, combined(): pl.pallas_call(functools.partial(combine_body, capacity=capacity, parts=p...  13 us
    pallas_call x2, Pallas kernels, summed_messages(): call(functools.partial(summed_body, capacity=capacity, parts=parts), (ste...  10.2 us
    pallas_call x2, Pallas kernels, side_rows(): call(sides_body, (steps,), [rows_of(hidden, 1), rows_of(hidden, 3), pl.Bl...  9.73 us
  transfers between devices with their start and end apart: 22, of which 9 were waited for; matrix products, arithmetic and copies ran while one was open for 6% of the time, Pallas kernels for 22%

commit v1 on v0

--- a/solution.py
+++ b/solution.py
@@ -8,7 +8,7 @@
 from jax.sharding import PartitionSpec as P
 
 
-RETURN_PIECES = 2
+PIECES = 2
 f32 = jnp.float32
 bf16 = jnp.bfloat16
 i32 = jnp.int32
@@ -48,10 +48,21 @@
     return jnp.where(picks, 1.0, 0.0).astype(bf16)
 
 
-def near_body(q_ref, code_ref, x_ref, gain_ref, out_ref, factor_ref, normed_ref, *, quarter, half):
+def spread_gain(gain_ref, wide_ref):
+    lanes = gain_ref.shape[1]
+    gain = gain_ref[...].astype(f32)
+    for k in range(gain_ref.shape[0]):
+        wide_ref[:, k * lanes : (k + 1) * lanes] = gain[k : k + 1, :]
+
+
+def near_body(q_ref, code_ref, x_ref, gain_ref, out_ref, factor_ref, normed_ref, wide_ref, *, quarter, half):
     step = pl.program_id(0)
     block, width = x_ref.shape
     side = out_ref.shape[1]
+
+    @pl.when(step == 0)
+    def _():
+        spread_gain(gain_ref, wide_ref)
 
     @pl.when(step < half)
     def _():
@@ -59,7 +70,7 @@
         factor = lax.rsqrt(jnp.sum(x * x, axis=1, keepdims=True) / width + 1e-06)
         factor_ref[...] = jnp.broadcast_to(factor, factor_ref.shape)
         columns = pl.ds(pl.multiple_of(q_ref[0] * quarter, quarter), side)
-        piece = x_ref[:, columns].astype(f32) * factor * gain_ref[:, columns].astype(f32)
+        piece = x_ref[:, columns].astype(f32) * factor * wide_ref[:, columns]
         normed_ref[pl.ds(step * block, block), :] = piece.astype(bf16)
 
     @pl.when(step >= half)
@@ -71,7 +82,7 @@
 def near_rows(index, code, x, gain, slots, side):
     rows, width = x.shape
     quarter = width // 4
-    half = 4
+    half = 2
     block, tile = rows // half, slots // half
     return call(
         functools.partial(near_body, quarter=quarter, half=half),
@@ -93,19 +104,23 @@
                 pl.BlockSpec((block, 128), lambda i, q: (jnp.minimum(i, half - 1), 0)),
             ),
         ],
-        [pltpu.VMEM((rows, side), bf16)],
+        [pltpu.VMEM((rows, side), bf16), pltpu.VMEM((1, width), f32)],
         2 * slots * rows * side,
         2 * (rows * width + slots * side),
     )(index, code, x, gain)
 
 
-def far_body(q_ref, code_ref, x0, x1, x2, x3, g0, g1, g2, g3, factor_ref, out_ref, normed_ref):
+def far_body(q_ref, code_ref, x0, x1, x2, x3, gain_ref, factor_ref, out_ref, normed_ref, wide_ref):
     @pl.when(pl.program_id(0) == 0)
     def _():
+        spread_gain(gain_ref, wide_ref)
+        quarter, rest = x0.shape[1], x1.shape[1]
         at = 0
-        for x_ref, gain_ref in ((x0, g0), (x1, g1), (x2, g2), (x3, g3)):
+        for x_ref, step in ((x0, 2), (x1, 0), (x2, 1), (x3, 3)):
             size = x_ref.shape[1]
-            piece = x_ref[...].astype(f32) * factor_ref[:, 0:1] * gain_ref[...].astype(f32)
+            start = (q_ref[0] + step) % 4 * quarter + quarter - size
+            gain = wide_ref[:, pl.ds(pl.multiple_of(start, rest), size)]
+            piece = x_ref[...].astype(f32) * factor_ref[:, 0:1] * gain
             normed_ref[:, at : at + size] = piece.astype(bf16)
             at += size
 
@@ -131,60 +146,142 @@
         (steps,),
         [whole(code.shape)]
         + [pl.BlockSpec((rows, size), place, pipeline_mode=once) for size, place in places]
-        + [pl.BlockSpec((1, size), place, pipeline_mode=once) for size, place in places]
-        + [whole(factor.shape)],
+        + [whole(gain.shape), whole(factor.shape)],
         [((slots, total), bf16, pl.BlockSpec((slots // steps, total), lambda i, q: (i, 0)))],
-        [pltpu.VMEM((rows, total), bf16)],
+        [pltpu.VMEM((rows, total), bf16), pltpu.VMEM((1, width), f32)],
         2 * slots * rows * total,
         2 * (rows + slots) * total,
-    )(index, code, x, x, x, x, gain, gain, gain, gain, factor)[0]
-
-
-def first_body(q_ref, x_ref, wg_ref, wu_ref, gate_ref, up_ref):
-    gate_ref[...] = dot(x_ref[...], wg_ref[...])
-    up_ref[...] = dot(x_ref[...], wu_ref[...])
-
-
-def first_part(index, x, wg, wu):
-    slots, side = x.shape
+    )(index, code, x, x, x, x, gain, factor)[0]
+
+
+def lent_block(rows, units, quarter, step):
+    return pl.BlockSpec(
+        (pl.Element(rows), pl.Element(units)),
+        lambda i, q: ((q[0] + step) % 4 * quarter, 0),
+        pipeline_mode=pl.Buffered(1),
+    )
+
+
+def first_body(q_ref, near_ref, wg_ref, wu_ref, gate_ref, up_ref):
+    gate_ref[...] = dot(near_ref[...], wg_ref[...])
+    up_ref[...] = dot(near_ref[...], wu_ref[...])
+
+
+def first_part(index, near, wg, wu):
+    slots, side = near.shape
     units = wg.shape[1]
     quarter = wg.shape[0] // 4
-    tile = slots // 4
-    weight = pl.BlockSpec(
-        (pl.Element(side), pl.Element(units)),
-        lambda i, q: (q[0] * quarter, 0),
-        pipeline_mode=pl.Buffered(1),
-    )
+    steps = 4
+    tile = slots // steps
     rowed = pl.BlockSpec((tile, units), lambda i, q: (i, 0))
     return call(
         first_body,
-        (4,),
-        [pl.BlockSpec((tile, side), lambda i, q: (i, 0)), weight, weight],
+        (steps,),
+        [pl.BlockSpec((tile, side), lambda i, q: (i, 0))] + [lent_block(side, units, quarter, 0)] * 2,
         [((slots, units), f32, rowed), ((slots, units), f32, rowed)],
         (),
         4 * slots * side * units,
         2 * slots * side + 4 * side * units + 8 * slots * units,
-    )(index, x, wg, wu)
-
-
-def hidden_body(q_ref, far_ref, right_ref, left_ref, gate_ref, up_ref, *refs, capacity):
-    weights, out_ref = refs[:-1], refs[-1]
-    many = len(weights) // 2
+    )(index, near, wg, wu)
+
+
+def second_body(q_ref, right_ref, left_ref, gate_ref, up_ref, gr, gl, ur, ul, gate_out, up_out):
+    right, left = right_ref[...], left_ref[...]
+    gate_out[...] = gate_ref[...] + dot(right, gr[...]) + dot(left, gl[...])
+    up_out[...] = up_ref[...] + dot(right, ur[...]) + dot(left, ul[...])
+
+
+def second_part(index, right, left, gate, up, wg, wu):
+    early, side = right.shape
+    units = wg.shape[1]
+    quarter = wg.shape[0] // 4
+    steps = 3
+    tile = early // steps
+    rowed = pl.BlockSpec((tile, units), lambda i, q: (i, 0))
+    lent = pl.BlockSpec((tile, side), lambda i, q: (i, 0))
+    weights = [lent_block(side, units, quarter, step) for step in (1, 3)]
+    return call(
+        second_body,
+        (steps,),
+        [lent, lent, rowed, rowed] + weights * 2,
+        [((early, units), f32, rowed), ((early, units), f32, rowed)],
+        (),
+        8 * early * side * units,
+        4 * early * side + 8 * side * units + 16 * early * units,
+    )(index, right, left, gate, up, wg, wg, wu, wu)
+
+
+def hidden_body(
+    q_ref,
+    far_ref,
+    right_ref,
+    left_ref,
+    gate_ref,
+    up_ref,
+    last_gate,
+    last_up,
+    wg_ref,
+    wu_ref,
+    out_ref,
+    both_ref,
+    far_weight,
+    lent_weight,
+    sems,
+    *,
+    capacity,
+):
+    step, last = pl.program_id(0), pl.num_programs(0) - 1
     parts, count, units = out_ref.shape
     size = parts * count
-
-    def total(start_ref, own):
-        value = start_ref[...] + dot(right_ref[...], own[0][...]) + dot(left_ref[...], own[1][...])
-        at = 0
-        for weight_ref in own[2:]:
-            rows = weight_ref.shape[0]
-            value += dot(far_ref[:, at : at + rows], weight_ref[...])
+    side = right_ref.shape[1]
+    quarter = wg_ref.shape[0] // 4
+    rest = quarter - side
+
+    def copies(weight, segments, first):
+        made, at = [], 0
+        for turn, skip, rows in segments:
+            start = pl.multiple_of((q_ref[0] + turn) % 4 * quarter + skip, rest)
+            for k, ref in enumerate((wg_ref, wu_ref)):
+                made.append(
+                    pltpu.make_async_copy(
+                        ref.at[pl.ds(start, rows), :],
+                        weight.at[pl.ds(at, rows), pl.ds(k * units, units)],
+                        sems.at[first + len(made)],
+                    )
+                )
             at += rows
-        return value
-
-    gate = total(gate_ref, weights[:many])
-    up = total(up_ref, weights[many:])
-    hidden = (gate / (1.0 + jnp.exp(-gate)) * up).astype(bf16)
+        return made
+
+    far_copies = copies(
+        far_weight, ((2, 0, quarter), (0, side, rest), (1, side, rest), (3, side, rest)), 0
+    )
+    lent_copies = copies(lent_weight, ((1, 0, side), (3, 0, side)), len(far_copies))
+
+    @pl.when(step == 0)
+    def _():
+        for copy in far_copies + lent_copies:
+            copy.start()
+        for copy in far_copies:
+            copy.wait()
+
+    both_ref[...] = dot(far_ref[...], far_weight[...])
+
+    @pl.when(step < last)
+    def _():
+        both_ref[:, :units] += gate_ref[...]
+        both_ref[:, units:] += up_ref[...]
+
+    @pl.when(step == last)
+    def _():
+        for copy in lent_copies:
+            copy.wait()
+        both_ref[...] += dot(right_ref[...], lent_weight[:side, :])
+        both_ref[...] += dot(left_ref[...], lent_weight[side:, :])
+        both_ref[:, :units] += last_gate[...]
+        both_ref[:, units:] += last_up[...]
+
+    gate = both_ref[:, :units]
+    hidden = (gate / (1.0 + jnp.exp(-gate)) * both_ref[:, units:]).astype(bf16)
     row = lax.broadcasted_iota(i32, (size, 1), 0)
     place = row % count // capacity * (parts * capacity) + row // count * capacity + row % capacity
     column = lax.broadcasted_iota(i32, (size, size), 1)
@@ -192,47 +289,29 @@
     out_ref[...] = dot(order, hidden).astype(bf16).reshape(parts, count, units)
 
 
-def hidden_units(index, far, right, left, gate, up, wg, wu, capacity):
-    slots, side = right.shape
+def hidden_units(index, far, right, left, sums, starts, wg, wu, capacity):
+    slots, depth = far.shape
+    tile, side = right.shape
     units = wg.shape[1]
-    quarter = wg.shape[0] // 4
-    rest = quarter - side
-    each = quarter // rest
-    steps, parts = 4, 4
-    tile = slots // steps
+    steps, parts = slots // tile, 4
     once = pl.Buffered(1)
-
-    def lent(step):
-        return pl.BlockSpec(
-            (pl.Element(side), pl.Element(units)),
-            lambda i, q: ((q[0] + step) % 4 * quarter, 0),
-            pipeline_mode=once,
-        )
-
-    def last(step):
-        return pl.BlockSpec(
-            (rest, units),
-            lambda i, q: ((q[0] + step) % 4 * each + each - 1, 0),
-            pipeline_mode=once,
-        )
-
-    weights = [
-        lent(1),
-        lent(3),
-        pl.BlockSpec((quarter, units), lambda i, q: ((q[0] + 2) % 4, 0), pipeline_mode=once),
-        last(0),
-        last(1),
-        last(3),
-    ]
-    depth = far.shape[1] + 2 * side
-
-    def rowed(size):
-        return pl.BlockSpec((tile, size), lambda i, q: (i, 0))
-
+    early = pl.BlockSpec((tile, units), lambda i, q: (jnp.minimum(i, steps - 2), 0))
+    late = pl.BlockSpec((tile, units), lambda i, q: (steps - 1, 0), pipeline_mode=once)
+    place = pl.BlockSpec(memory_space=pl.ANY)
     return call(
         functools.partial(hidden_body, capacity=capacity),
         (steps,),
-        [rowed(far.shape[1]), rowed(side), rowed(side), rowed(units), rowed(units)] + weights * 2,
+        [
+            pl.BlockSpec((tile, depth), lambda i, q: (i, 0)),
+            whole(right.shape),
+            whole(left.shape),
+            early,
+            early,
+            late,
+            late,
+            place,
+            place,
+        ],
         [
             (
                 (parts, slots // parts, units),
@@ -240,10 +319,15 @@
                 pl.BlockSpec((parts, tile // parts, units), lambda i, q: (0, i, 0)),
             )
         ],
-        (),
-        4 * slots * depth * units,
+        [
+            pltpu.VMEM((tile, 2 * units), f32),
+            pltpu.VMEM((depth, 2 * units), bf16),
+            pltpu.VMEM((2 * side, 2 * units), bf16),
+            pltpu.SemaphoreType.DMA((12,)),
+        ],
+        4 * slots * depth * units + 8 * tile * side * units,
         2 * slots * depth + 4 * depth * units + 10 * slots * units,
-    )(index, far, right, left, gate, up, *[wg] * 6, *[wu] * 6)[0]
+    )(index, far, right, left, *sums, *starts, wg, wu)[0]
 
 
 def rows_of(hidden, step):
@@ -254,14 +338,16 @@
 
 
 def sides_body(q_ref, to_right_ref, to_left_ref, down_ref, right_ref, left_ref):
-    right_ref[...] = dot(to_right_ref[...], down_ref[...]).astype(bf16)
-    left_ref[...] = dot(to_left_ref[...], down_ref[...]).astype(bf16)
+    count = to_right_ref.shape[0]
+    value = dot(jnp.concatenate([to_right_ref[...], to_left_ref[...]], axis=0), down_ref[...])
+    right_ref[...] = value[:count].astype(bf16)
+    left_ref[...] = value[count:].astype(bf16)
 
 
 def side_rows(index, hidden, down, piece, pieces):
     _, count, units = hidden.shape
     width = down.shape[1] // pieces
-    steps = 4
+    steps = 2
     tile = width // steps
     tiled = pl.BlockSpec((count, tile), lambda i, q: (0, i))
     return call(
@@ -286,15 +372,13 @@
 def own_rows(index, hidden, down, piece, pieces):
     _, count, units = hidden.shape
     width = down.shape[1] // pieces
-    steps = 4
+    steps = 2
     tile = width // steps
     return call(
         own_body,
         (steps,),
-        [
-            rows_of(hidden, 0),
-            pl.BlockSpec((units, tile), lambda i, q: (0, piece * steps + i)),
-        ],
+        [rows_of(hidden, 0)]
+        + [pl.BlockSpec((units, tile), lambda i, q: (0, piece * steps + i))],
         [((count, width), bf16, pl.BlockSpec((count, tile), lambda i, q: (0, i)))],
         (),
         2 * count * units * width,
@@ -302,20 +386,24 @@
     )(index, hidden, down)[0]
 
 
-def messages_of(value, fold, capacity, parts):
-    many = value.shape[0]
+def order_of(many, capacity, parts):
     size, each = many * parts, parts * capacity
     row = lax.broadcasted_iota(i32, (size, 1), 0)
     place = row % each // capacity * many + row // each * capacity + row % capacity
     column = lax.broadcasted_iota(i32, (size, size), 1)
-    order = jnp.where(column == place, 1.0, 0.0).astype(bf16)
+    return jnp.where(column == place, 1.0, 0.0).astype(bf16)
+
+
+def messages_of(order, value, fold, parts):
     stack = jnp.concatenate([value[:, k * fold : (k + 1) * fold] for k in range(parts)], axis=0)
     return dot(order, stack).astype(bf16)
 
 
 def across_body(q_ref, rows_ref, down_ref, out_ref, value_ref, *, capacity, parts, steps):
     step = pl.program_id(0)
-    tile, fold, many = down_ref.shape[1], out_ref.shape[1], out_ref.shape[0] // parts
+    tile, fold = down_ref.shape[1], out_ref.shape[1]
+    groups = 2
+    many = out_ref.shape[0] // (parts * groups)
 
     @pl.when(step < steps)
     def _():
@@ -324,25 +412,25 @@
 
     @pl.when(step >= steps)
     def _():
-        value = value_ref[pl.ds(pl.multiple_of((step - steps) * many, many), many), :]
-        out_ref[...] = messages_of(value, fold, capacity, parts)
-
-
-def across_messages(index, hidden, down, piece, pieces, capacity):
+        order = order_of(many, capacity, parts)
+        size = many * parts
+        for g in range(groups):
+            start = pl.multiple_of(((step - steps) * groups + g) * many, many)
+            value = value_ref[pl.ds(start, many), :]
+            out_ref[g * size : (g + 1) * size, :] = messages_of(order, value, fold, parts)
+
+
+def across_messages(index, hidden, down, capacity):
     parts, count, units = hidden.shape
-    width = down.shape[1] // pieces
+    width = down.shape[1]
     slots, fold = parts * count, width // parts
-    steps = 4
+    steps = 2
     tile = width // steps
     return call(
         functools.partial(across_body, capacity=capacity, parts=parts, steps=steps),
         (2 * steps,),
-        [
-            rows_of(hidden, 2),
-            pl.BlockSpec(
-                (units, tile), lambda i, q: (0, piece * steps + jnp.minimum(i, steps - 1))
-            ),
-        ],
+        [rows_of(hidden, 2)]
+        + [pl.BlockSpec((units, tile), lambda i, q: (0, jnp.minimum(i, steps - 1)))],
         [
             (
                 (slots, fold),
@@ -357,14 +445,22 @@
 
 
 def summed_body(q_ref, own_ref, left_ref, right_ref, out_ref, *, capacity, parts):
-    total = own_ref[...].astype(f32) + left_ref[...].astype(f32) + right_ref[...].astype(f32)
-    out_ref[...] = messages_of(total.astype(bf16), out_ref.shape[1], capacity, parts)
+    groups = 2
+    fold = out_ref.shape[1]
+    size = out_ref.shape[0] // groups
+    many = size // parts
+    order = order_of(many, capacity, parts)
+    for g in range(groups):
+        part = slice(g * many, (g + 1) * many)
+        total = own_ref[part, :].astype(f32) + left_ref[part, :].astype(f32)
+        total = (total + right_ref[part, :].astype(f32)).astype(bf16)
+        out_ref[g * size : (g + 1) * size, :] = messages_of(order, total, fold, parts)
 
 
 def summed_messages(index, own, left, right, capacity, parts):
     count, width = own.shape
     slots, fold = count * parts, width // parts
-    steps = 4
+    steps = 2
     rowed = pl.BlockSpec((count // steps, width), lambda i, q: (i, 0))
     return call(
         functools.partial(summed_body, capacity=capacity, parts=parts),
@@ -512,6 +608,7 @@
     slots = sources * per_source
     quarter = width // parts
     side = 7 * quarter // 8
+    early = 3 * slots // 4
 
     ids = expert_ids.T.reshape(chosen, parts, block)
     earlier = jnp.arange(block)[:, None] < jnp.arange(block)[None, :]
@@ -527,15 +624,17 @@
 
     taps = mixer_taps.shape[0]
     length = mixer_value.shape[0]
+    last_value, last_gate = mixer_value[length - (taps - 1) :], mixer_gate[length - (taps - 1) :]
+    last = (last_value.astype(f32) * jax.nn.sigmoid(last_gate.astype(f32))).astype(bf16)
+    before = lax.ppermute(last, "ep", [(i, i + 1) for i in range(sources - 1)])
+
+    gain = routed_gain.reshape(-1, 128)
+    near, factor = near_rows(index, code, routed_input, gain, slots, side)
+    near, before, mixer_value, mixer_gate, mixer_taps = lax.optimization_barrier(
+        (near, before, mixer_value, mixer_gate, mixer_taps)
+    )
+    near = exchanged(near)
     gated = (mixer_value.astype(f32) * jax.nn.sigmoid(mixer_gate.astype(f32))).astype(bf16)
-    before = lax.ppermute(
-        gated[length - (taps - 1) :], "ep", [(i, i + 1) for i in range(sources - 1)]
-    )
-
-    gain = routed_gain.reshape(1, width)
-    near, factor = near_rows(index, code, routed_input, gain, slots, side)
-    near, before = lax.optimization_barrier((near, before))
-    near = exchanged(near)
 
     extended = jnp.concatenate([before, gated], axis=0).astype(f32)
     taps_float = mixer_taps.astype(f32)
@@ -561,15 +660,11 @@
 
     factor, right_low, left_high = lax.optimization_barrier((factor, right_low, left_high))
     far = far_rows(index, code, routed_input, gain, factor, slots, side)
-    from_left, from_right = turned(near, "tp", 1), turned(near, "tp", -1)
+    lent = []
+    for piece in (near[:early], near[early:]):
+        lent.append((turned(piece, "tp", -1), turned(piece, "tp", 1)))
     far = exchanged(far)
 
-    gate, up = first_part(index, near, gate_weight[0], up_weight[0])
-    hidden = hidden_units(
-        index, far, from_right, from_left, gate, up, gate_weight[0], up_weight[0], capacity
-    )
-
-    hidden, right_low, left_high = lax.optimization_barrier((hidden, right_low, left_high))
     sum_low = turned((right_low.astype(f32) + via_right.astype(f32)).astype(bf16), "tp", 1)
     sum_high = turned((left_high.astype(f32) + via_left.astype(f32)).astype(bf16), "tp", -1)
     middle = width // 2
@@ -581,6 +676,12 @@
         axis=1,
     ).astype(bf16)
 
+    weights = (gate_weight[0], up_weight[0])
+
+    starts = first_part(index, near, *weights)
+    sums = second_part(index, *lent[0], *starts, *weights)
+    hidden = hidden_units(index, far, *lent[1], sums, starts, *weights, capacity)
+
     def home_of(which):
         own_ids = lax.dynamic_slice_in_dim(ids, which, 1, 1)[:, 0]
         own_rank = lax.dynamic_slice_in_dim(rank, which, 1, 1)[:, 0]
@@ -589,24 +690,21 @@
 
     down = down_weight[0]
     far_home, own_home = home_of(across), home_of(q)
-    pieces = RETURN_PIECES
     got = []
-    for piece in range(pieces):
-        to_right, to_left = side_rows(index, hidden, down, piece, pieces)
+    for piece in range(PIECES):
+        to_right, to_left = side_rows(index, hidden, down, piece, PIECES)
         got.append((turned(to_right, "tp", 1), turned(to_left, "tp", -1)))
-    messages = across_messages(index, hidden, down, 0, 1, capacity)
+    messages = across_messages(index, hidden, down, capacity)
     far_back = exchanged(messages)
+    own = [own_rows(index, hidden, down, piece, PIECES) for piece in range(PIECES)]
     extra = combined(index, *far_home, far_back, capacity, parts)
-    own = [own_rows(index, hidden, down, piece, pieces) for piece in range(pieces)]
     extra, own[-1] = lax.optimization_barrier((extra, own[-1]))
     extra = turned(extra, "tp", 2)
     result = None
-    for piece in range(pieces):
+    for piece in range(PIECES):
         messages = summed_messages(index, own[piece], *got[piece], capacity, parts)
         back = exchanged(messages)
-        result = combined(
-            index, *own_home, back, capacity, parts, extra, result, piece, pieces
-        )
+        result = combined(index, *own_home, back, capacity, parts, extra, result, piece, PIECES)
     return (mixer_result, result)
 
 

time: 290 us -> 280 us (0.966)
  waiting for transfers between devices: 110 us -> 95.4 us
  starting transfers between devices: 60 us -> 64.8 us
    all_to_all x5, waiting for transfers between devices: 41.9 us -> 3.13 us  [exchanged(): return lax.all_to_all(messages, 'ep', 0, 0, tiled=True).reshape(slots, size)]
    ppermute x16 -> x18, waiting for transfers between devices: 67.8 us -> 92.2 us  [turned(): lax.ppermute(value, axis, [(i, (i + steps) % count) for i in range(count)])]
    ppermute x16 -> x18, starting transfers between devices: 21.7 us -> 26.3 us  [turned(): lax.ppermute(value, axis, [(i, (i + steps) % count) for i in range(count)])]
    pallas_call x4 -> x5, Pallas kernels: 32.9 us -> 36.4 us  [the longest x1 14.6 us: hidden_units(): call(functools.partial(hidden_body, capacity=capacity), (steps,), [pl.Blo...]
  transfers between devices with their start and end apart: 22 -> 24, of which waited for: 9 -> 11; matrix products, arithmetic and copies ran while one was open for 6% -> 8% of each run, Pallas kernels for 22% -> 24%
where the time goes in v1:
time: 280 us; the launch traced here: 279 us
  waiting for transfers between devices  95.4 us (34%)
  Pallas kernels  91.2 us (33%)
  starting transfers between devices  64.8 us (23%)
  other arithmetic  18.1 us (6%)
  local copies, waits for them, and re-layouts  8.45 us (3%)
    ppermute x18, waiting for transfers between devices, turned(): lax.ppermute(value, axis, [(i, (i + steps) % count) for i in range(count)])  92.2 us
    all_to_all x5, starting transfers between devices, exchanged(): return lax.all_to_all(messages, 'ep', 0, 0, tiled=True).reshape(slots, size)  37.2 us
    ppermute x18, starting transfers between devices, turned(): lax.ppermute(value, axis, [(i, (i + steps) % count) for i in range(count)])  26.3 us
    pallas_call x1, Pallas kernels, hidden_units(): call(functools.partial(hidden_body, capacity=capacity), (steps,), [pl.Blo...  14.6 us
    pallas_call x3, Pallas kernels, combined(): pl.pallas_call(functools.partial(combine_body, capacity=capacity, parts=p...  13 us
    pallas_call x1, Pallas kernels, second_part(): call(second_body, (steps,), [lent, lent, rowed, rowed] + weights * 2, [((...  8.86 us
    pallas_call x2, Pallas kernels, side_rows(): call(sides_body, (steps,), [rows_of(hidden, 1), rows_of(hidden, 3), pl.Bl...  8.3 us
    pallas_call x2, Pallas kernels, summed_messages(): call(functools.partial(summed_body, capacity=capacity, parts=parts), (ste...  8.07 us
  transfers between devices with their start and end apart: 24, of which 11 were waited for; matrix products, arithmetic and copies ran while one was open for 8% of the time, Pallas kernels for 24%

profile of v1, /device:TPU:0, one launch (start us, length us, event | category | flops | bytes accessed | tf_op | source)
XLA Modules:
  0.0 278.8 jit_solution(4521766747353425404)
XLA Ops:
  0.6 0.8 multiply_convert_fusion.2
  1.4 1.3 collective-permute-start
  2.9 0.8 copy.21
  4.0 1.3 bitcast_add_fusion.code_ref
  5.3 5.9 %shard_map.131 = (bf16[1280,896]{1,0:T(8,128)(2,1)}, f32[512,128]{1,0:T(8,128)}) custom-call(s32[1]{0:T(128)} %bitcast.q_ref, s32[2,512]{1,0:T(2,128)} %bitcast_add_fusion.code_ref, bf16[512,4096]{1,0:T(8,128)(2,1)} %x3.1, bf16[32,128]{1,0:T(8,128)(2,1)} %bitcast.102), custom_call_target="tpu_custom_call" | custom-call | flops 1174405120 | bytes 6488064 | tf_op jit(solution)/shard_map/pallas_call | solution.py:87
  11.3 10.2 %all-to-all-start.1 = ((bf16[32,40,896]{2,1,0:T(8,128)(2,1)}), bf16[32,40,896]{2,1,0:T(8,128)(2,1)S(1)}, u32[]{:S(2)}, u32[]{:S(2)}) async-start(bf16[32,40,896]{2,1,0:T(8,128)(2,1)} %bitcast.89), calls=%async_computation.1 | async-start | bytes 4587520 | tf_op jit(solution)/shard_map/all_to_all | solution.py:623
  21.5 1.3 multiply_convert_fusion.1
  23.0 5.0 %fusion.30 = (f32[512]{0:T(512)S(1)}, f32[512]{0:T(512)S(1)}, f32[512,512]{1,0:T(8,128)S(1)}) fusion(f32[542,512]{1,0:T(8,128)S(1)} %maximum_convert_fusion, f32[512]{0:T(512)S(1)} %bitcast.115, f32[512]{0:T(512)S(1)} %bitcast.114, f32[512]{0:T(512)S(1)} %bitcast.113, f32[512]{0:T(512)S(1)} %bitcast.112, f32[512]{0:T(512)S(1)} %bitcast.111, ...), kind=kLoop, calls=%fused_computation.87 | loop fusion | flops 16776192 | bytes 33622016 | tf_op jit(solution)/shard_map/reduce_sum | solution.py:644
  28.1 2.8 %collective-permute-start.2 = (f32[2,512]{1,0:T(2,128)S(1)}, f32[2,512]{1,0:T(2,128)S(1)}, u32[]{:S(2)}, u32[]{:S(2)}) collective-permute-start(f32[2,512]{1,0:T(2,128)S(1)} %pad_maximum_fusion.1), channel_id=1, source_target_pairs={{0,3},{1,0},{2,1},{3,2},{4,7},{5,4},{6,5},{7,6},{8,11},{9,8},{10,9... | collective-permute-start | bytes 12296 | tf_op jit(solution)/shard_map/ppermute | solution.py:19
  30.9 0.8 collective-permute-start.3
  31.7 0.9 collective-permute-start.1
  32.6 3.4 %collective-permute-done.3 = f32[2,512]{1,0:T(2,128)S(1)} collective-permute-done((f32[2,512]{1,0:T(2,128)S(1)}, f32[2,512]{1,0:T(2,128)S(1)}, u32[]{:S(2)}, u32[]{:S(2)}) %collective-permute-start.3) | collective-permute-done | bytes 4128 | tf_op jit(solution)/shard_map/ppermute | solution.py:19
  36.6 1.2 multiply_convert_fusion.hidden_ref
  37.8 7.0 %shard_map.132 = (bf16[128,4096]{1,0:T(8,128)(2,1)}, bf16[128,2048]{1,0:T(8,128)(2,1)}, bf16[128,2048]{1,0:T(8,128)(2,1)}, bf16[128,2048]{1,0:T(8,128)(2,1)}, bf...) custom-call(s32[1]{0:T(128)} %bitcast.q_ref, ...), custom_call_target="tpu_custom_call" | custom-call | flops 2147483648 | bytes 8912896 | tf_op jit(solution)/shard_map/pallas_call | solution.py:572
  44.8 6.0 %shard_map.133 = bf16[1280,1408]{1,0:T(8,128)(2,1)} custom-call(s32[1]{0:T(128)} %bitcast.q_ref, s32[2,512]{1,0:T(2,128)} %bitcast_add_fusion.code_ref, bf16[512,4096]{1,0:T(8,128)(2,1)} %x3.1, bf16[512,4096]{1,0:T(8,128)(2,1)} %x3.1, bf16[512,4096]{1,0:T(8,128)(2,1)} %x3.1, bf16[512,4096]{1,0:T(8,128)(2,1)} %x3.1, bf16[32,128]{1,0:T(8,128)(2,1)} %bitcast.103, ...), custom_call_target="tpu_custom_call" | custom-call | flops 1845493760 | bytes 5046272 | tf_op jit(solution)/shard_map/pallas_call | solution.py:144
  50.7 3.1 %all-to-all-done.1 = bf16[32,40,896]{2,1,0:T(8,128)(2,1)S(1)} async-done(((bf16[32,40,896]{2,1,0:T(8,128)(2,1)}), bf16[32,40,896]{2,1,0:T(8,128)(2,1)S(1)}, u32[]{:S(2)}, u32[]{:S(2)}) %all-to-all-start.1) | async-done | bytes 2293792 | tf_op jit(solution)/shard_map/all_to_all | solution.py:623
  53.8 4.8 %all-to-all-start = ((bf16[32,40,1408]{2,1,0:T(8,128)(2,1)}), bf16[32,40,1408]{2,1,0:T(8,128)(2,1)}, u32[]{:S(2)}, u32[]{:S(2)}) async-start(bf16[32,40,1408]{2,1,0:T(8,128)(2,1)} %bitcast.82), calls=%async_computation | async-start | bytes 7208960 | tf_op jit(solution)/shard_map/all_to_all | solution.py:623
  58.7 1.3 slice.353
  60.0 1.5 collective-permute-start.13
  61.5 1.7 collective-permute-start.12
  63.7 2.9 %collective-permute-start.10 = (bf16[320,896]{1,0:T(8,128)(2,1)S(1)}, bf16[320,896]{1,0:T(8,128)(2,1)S(1)}, u32[]{:S(2)}, u32[]{:S(2)}) collective-permute-start(bf16[320,896]{1,0:T(8,128)(2,1)S(1)} %bitcast.93), channel_id=1, source_target_pairs={{0,3},{1,0},{2,1},{3,2},{4,7},{5,4},{6,5},{7,6},{8,11},{9,8},{10,9... | collective-permute-start | bytes 1720328 | tf_op jit(solution)/shard_map/ppermute | solution.py:19
  66.6 6.4 %shard_map.134 = (f32[1280,512]{1,0:T(8,128)}, f32[1280,512]{1,0:T(8,128)}) custom-call(s32[1]{0:T(128)} %bitcast.q_ref, bf16[1280,896]{1,0:T(8,128)(2,1)} %bitcast.81, bf16[4096,512]{1,0:T(8,128)(2,1)} %bitcast.73, bf16[4096,512]{1,0:T(8,128)(2,1)} %bitcast.77), custom_call_target="tpu_custom_call" | custom-call | flops 2348810240 | bytes 9371648 | tf_op jit(solution)/shard_map/pallas_call | solution.py:177
  73.0 28.9 %collective-permute-done.13.left_ref = bf16[960,896]{1,0:T(8,128)(2,1)} collective-permute-done((bf16[960,896]{1,0:T(8,128)(2,1)}, bf16[960,896]{1,0:T(8,128)(2,1)}, u32[]{:S(2)}, u32[]{:S(2)}) %collective-permute-start.13) | collective-permute-done | bytes 1720352 | tf_op jit(solution)/shard_map/ppermute | solution.py:19
  102.3 8.9 %shard_map.135 = (f32[960,512]{1,0:T(8,128)}, f32[960,512]{1,0:T(8,128)}) custom-call(s32[1]{0:T(128)} %bitcast.q_ref, bf16[960,896]{1,0:T(8,128)(2,1)} %collective-permute-done.12.right_ref, bf16[960,896]{1,0:T(8,128)(2,1)} %collective-permute-done.13.left_ref, f32[1280,512]{1,0:T(8,128)} %get-tuple-element.46.gate_ref.last_gate, ...), custom_call_target="tpu_custom_call" | custom-call | flops 3523215360 | bytes 14974976 | tf_op jit(solution)/shard_map/pallas_call | solution.py:203
  111.1 2.2 collective-permute-done.11.left_ref
  113.3 0.8 copy-done.5
  114.3 14.6 %shard_map.136.rows_ref.to_right_ref.to_left_ref = bf16[4,320,512]{2,1,0:T(8,128)(2,1)} custom-call(s32[1]{0:T(128)} %bitcast.q_ref, bf16[1280,1408]{1,0:T(8,128)(2,1)} %bitcast.45.far_ref, bf16[320,896]{1,0:T(8,128)(2,1)} %copy-done.6, bf16[320,896]{1,0:T(8,128)(2,1)} %copy-done.5, f32[960,512]{1,0:T(8,128)} %get-tuple-element.48.gate_ref, ...), custom_call_target="tpu_custom_call" | custom-call | flops 4865392640 | bytes 13041664 | tf_op jit(solution)/shard_map/pallas_call | solution.py:301
  128.9 6.6 %shard_map.137 = bf16[1280,1024]{1,0:T(8,128)(2,1)} custom-call(s32[1]{0:T(128)} %bitcast.q_ref, bf16[4,320,512]{2,1,0:T(8,128)(2,1)} %shard_map.136.rows_ref.to_right_ref.to_left_ref, bf16[512,4096]{1,0:T(8,128)(2,1)} %bitcast.68), custom_call_target="tpu_custom_call" | custom-call | flops 1342177280 | bytes 7143424 | tf_op jit(solution)/shard_map/pallas_call | solution.py:429
  135.5 7.3 %all-to-all-start.2 = ((bf16[32,40,1024]{2,1,0:T(8,128)(2,1)}), bf16[32,40,1024]{2,1,0:T(8,128)(2,1)S(1)}, u32[]{:S(2)}, u32[]{:S(2)}) async-start(bf16[32,40,1024]{2,1,0:T(8,128)(2,1)} %bitcast.83), calls=%async_computation.2 | async-start | bytes 5242880 | tf_op jit(solution)/shard_map/all_to_all | solution.py:623
  142.9 4.2 %shard_map.142 = (bf16[320,2048]{1,0:T(8,128)(2,1)}, bf16[320,2048]{1,0:T(8,128)(2,1)}) custom-call(s32[1]{0:T(128)} %bitcast.q_ref, bf16[4,320,512]{2,1,0:T(8,128)(2,1)} %shard_map.136.rows_ref.to_right_ref.to_left_ref, bf16[4,320,512]{2,1,0:T(8,128)(2,1)} %shard_map.136.rows_ref.to_right_ref.to_left_ref, bf16[512,4096]{1,0:T(8,128)(2,1)} %bitcast.69), custom_call_target="tpu_custom_call" | custom-call | flops 1342177280 | bytes 5373952 | tf_op jit(solution)/shard_map/pallas_call | solution.py:353
  147.1 1.3 collective-permute-start.17
  148.4 1.9 collective-permute-start.18
  150.4 4.1 %shard_map.139 = (bf16[320,2048]{1,0:T(8,128)(2,1)}, bf16[320,2048]{1,0:T(8,128)(2,1)}) custom-call(s32[1]{0:T(128)} %bitcast.q_ref, bf16[4,320,512]{2,1,0:T(8,128)(2,1)} %shard_map.136.rows_ref.to_right_ref.to_left_ref, bf16[4,320,512]{2,1,0:T(8,128)(2,1)} %shard_map.136.rows_ref.to_right_ref.to_left_ref, bf16[512,4096]{1,0:T(8,128)(2,1)} %bitcast.70), custom_call_target="tpu_custom_call" | custom-call | flops 1342177280 | bytes 5373952 | tf_op jit(solution)/shard_map/pallas_call | solution.py:353
  154.5 1.2 collective-permute-start.14
  156.0 0.7 add_bitcast_fusion
  156.6 2.0 collective-permute-start.6
  158.7 3.3 %shard_map.141.own_ref = bf16[320,2048]{1,0:T(8,128)(2,1)} custom-call(s32[1]{0:T(128)} %bitcast.q_ref, bf16[4,320,512]{2,1,0:T(8,128)(2,1)} %shard_map.136.rows_ref.to_right_ref.to_left_ref, bf16[512,4096]{1,0:T(8,128)(2,1)} %bitcast.71), custom_call_target="tpu_custom_call" | custom-call | flops 671088640 | bytes 3735552 | tf_op jit(solution)/shard_map/pallas_call | solution.py:377
  161.9 18.3 %collective-permute-done.17.left_ref = bf16[320,2048]{1,0:T(8,128)(2,1)} collective-permute-done((bf16[320,2048]{1,0:T(8,128)(2,1)}, bf16[320,2048]{1,0:T(8,128)(2,1)}, u32[]{:S(2)}, u32[]{:S(2)}) %collective-permute-start.17) | collective-permute-done | bytes 1310752 | tf_op jit(solution)/shard_map/ppermute | solution.py:19
  180.2 1.5 collective-permute-start.7
  181.8 1.7 collective-permute-start.15
  183.5 4.0 %shard_map.143 = bf16[1280,512]{1,0:T(8,128)(2,1)} custom-call(s32[1]{0:T(128)} %bitcast.q_ref, bf16[320,2048]{1,0:T(8,128)(2,1)} %shard_map.141.own_ref, bf16[320,2048]{1,0:T(8,128)(2,1)} %collective-permute-done.17.left_ref, bf16[320,2048]{1,0:T(8,128)(2,1)} %collective-permute-done.18.right_ref), custom_call_target="tpu_custom_call" | custom-call | flops 419430400 | bytes 5242880 | tf_op jit(solution)/shard_map/pallas_call | solution.py:465
  187.5 3.9 %collective-permute-done.4 = bf16[128,2048]{1,0:T(8,128)(2,1)S(1)} collective-permute-done((bf16[128,2048]{1,0:T(8,128)(2,1)}, bf16[128,2048]{1,0:T(8,128)(2,1)S(1)}, u32[]{:S(2)}, u32[]{:S(2)}) %collective-permute-start.4) | collective-permute-done | bytes 524320 | tf_op jit(solution)/shard_map/ppermute | solution.py:19
  191.5 0.7 copy-done.8
  192.2 1.5 copy-done.3
  193.6 7.4 %all-to-all-start.4 = ((bf16[32,40,512]{2,1,0:T(8,128)(2,1)}), bf16[32,40,512]{2,1,0:T(8,128)(2,1)S(1)}, u32[]{:S(2)}, u32[]{:S(2)}) async-start(bf16[32,40,512]{2,1,0:T(8,128)(2,1)} %bitcast.86), calls=%async_computation.4 | async-start | bytes 2621440 | tf_op jit(solution)/shard_map/all_to_all | solution.py:623
  201.0 2.1 add_convert_fusion.3
  203.2 0.8 collective-permute-start.5
  204.0 2.0 add_convert_fusion.1
  206.0 13.6 %collective-permute-done.14.left_ref = bf16[320,2048]{1,0:T(8,128)(2,1)} collective-permute-done((bf16[320,2048]{1,0:T(8,128)(2,1)}, bf16[320,2048]{1,0:T(8,128)(2,1)}, u32[]{:S(2)}, u32[]{:S(2)}) %collective-permute-start.14) | collective-permute-done | bytes 1310752 | tf_op jit(solution)/shard_map/ppermute | solution.py:19
  219.6 1.5 collective-permute-start.8
  221.1 0.7 copy.31.share_ref
  221.9 3.2 %shard_map.138.own_ref = bf16[320,2048]{1,0:T(8,128)(2,1)} custom-call(s32[1]{0:T(128)} %bitcast.q_ref, bf16[4,320,512]{2,1,0:T(8,128)(2,1)} %shard_map.136.rows_ref.to_right_ref.to_left_ref, bf16[512,4096]{1,0:T(8,128)(2,1)} %bitcast.72), custom_call_target="tpu_custom_call" | custom-call | flops 671088640 | bytes 3735552 | tf_op jit(solution)/shard_map/pallas_call | solution.py:377
  225.0 4.9 %combined.3 = bf16[128,4096]{1,0:T(8,128)(2,1)} custom-call(s32[1]{0:T(128)} %bitcast.q_ref, s32[128,2]{1,0:T(8,128)} %get-tuple-element.61.home_ref, f32[128,2]{1,0:T(8,128)} %copy.31.share_ref, bf16[1280,1024]{1,0:T(8,128)(2,1)} %bitcast.88), custom_call_target="tpu_custom_call" | custom-call | flops 1342177280 | bytes 4718592 | tf_op jit(solution)/shard_map/combined/pallas_call | solution.py:519
  230.0 0.9 collective-permute-done.15.right_ref
  230.9 4.0 %shard_map.140 = bf16[1280,512]{1,0:T(8,128)(2,1)} custom-call(s32[1]{0:T(128)} %bitcast.q_ref, bf16[320,2048]{1,0:T(8,128)(2,1)} %shard_map.138.own_ref, bf16[320,2048]{1,0:T(8,128)(2,1)} %collective-permute-done.14.left_ref, bf16[320,2048]{1,0:T(8,128)(2,1)} %collective-permute-done.15.right_ref), custom_call_target="tpu_custom_call" | custom-call | flops 419430400 | bytes 5242880 | tf_op jit(solution)/shard_map/pallas_call | solution.py:465
  235.0 7.4 %all-to-all-start.3 = ((bf16[32,40,512]{2,1,0:T(8,128)(2,1)}), bf16[32,40,512]{2,1,0:T(8,128)(2,1)S(1)}, u32[]{:S(2)}, u32[]{:S(2)}) async-start(bf16[32,40,512]{2,1,0:T(8,128)(2,1)} %bitcast.87), calls=%async_computation.3 | async-start | bytes 2621440 | tf_op jit(solution)/shard_map/all_to_all | solution.py:623
  242.4 3.0 %collective-permute-start.16 = (bf16[128,4096]{1,0:T(8,128)(2,1)}, bf16[128,4096]{1,0:T(8,128)(2,1)}, u32[]{:S(2)}, u32[]{:S(2)}) collective-permute-start(bf16[128,4096]{1,0:T(8,128)(2,1)} %combined.3), channel_id=1, source_target_pairs={{0,2},{1,3},{2,0},{3,1},{4,6},{5,7},{6,4},{7,5},{8,10},{9,11},{10,... | collective-permute-start | bytes 3145736 | tf_op jit(solution)/shard_map/ppermute | solution.py:19
  245.3 0.7 copy.29.share_ref
  246.1 2.2 add_convert_fusion.2
  248.3 1.0 pad_maximum_fusion
  249.4 20.2 %collective-permute-done.16.refs_0_ = bf16[128,4096]{1,0:T(8,128)(2,1)} collective-permute-done((bf16[128,4096]{1,0:T(8,128)(2,1)}, bf16[128,4096]{1,0:T(8,128)(2,1)}, u32[]{:S(2)}, u32[]{:S(2)}) %collective-permute-start.16) | collective-permute-done | bytes 1048608 | tf_op jit(solution)/shard_map/ppermute | solution.py:19
  269.6 4.0 %combined.4.refs_1_ = bf16[128,4096]{1,0:T(8,128)(2,1)} custom-call(s32[1]{0:T(128)} %bitcast.q_ref, s32[128,2]{1,0:T(8,128)} %get-tuple-element.62.home_ref, f32[128,2]{1,0:T(8,128)} %copy.29.share_ref, bf16[1280,512]{1,0:T(8,128)(2,1)} %bitcast.85, bf16[128,4096]{1,0:T(8,128)(2,1)} %collective-permute-done.16.refs_0_), custom_call_target="tpu_custom_call" | custom-call | flops 671088640 | bytes 2359296 | tf_op jit(solution)/shard_map/combined/pallas_call | solution.py:519
  273.6 1.1 copy-done.1
  274.7 4.0 %combined.5 = bf16[128,4096]{1,0:T(8,128)(2,1)} custom-call(s32[1]{0:T(128)} %bitcast.q_ref, s32[128,2]{1,0:T(8,128)} %get-tuple-element.62.home_ref, f32[128,2]{1,0:T(8,128)} %copy.29.share_ref, bf16[1280,512]{1,0:T(8,128)(2,1)} %bitcast.84, bf16[128,4096]{1,0:T(8,128)(2,1)} %collective-permute-done.16.refs_0_, ...), custom_call_target="tpu_custom_call", output_to_operand_aliasing={{}: (5, {})} | custom-call | flops 671088640 | bytes 2359296 | tf_op jit(solution)/shard_map/combined/pallas_call | solution.py:519
  (56 shorter events, 2.6 us)
Async XLA Ops:
  1.4 9.7 %collective-permute-start = (bf16[30,512]{1,0:T(8,128)(2,1)S(1)}, bf16[30,512]{1,0:T(8,128)(2,1)S(1)}, u32[]{:S(2)}, u32[]{:S(2)}) collective-permute-start(bf16[30,512]{1,0:T(8,128)(2,1)S(1)} %multiply_convert_fusion.2), channel_id=1, source_target_pairs={{0,4},{4,8},{8,12},{12,16},{16,20},{20,24},{24,28},{28,32},{32,36}... | collective-permute-start | bytes 92168 | tf_op jit(solution)/shard_map/ppermute | solution.py:629
  5.3 5.9 %copy-start.9 = (bf16[31,512]{1,0:T(8,128)(2,1)S(1)}, bf16[31,512]{1,0:T(8,128)(2,1)}, u32[]{:S(2)}) copy-start(bf16[31,512]{1,0:T(8,128)(2,1)} %param.14) | copy-start | bytes 95236
  11.3 10.2 %copy-start.4 = (bf16[512,512]{1,0:T(8,128)(2,1)S(1)}, bf16[512,512]{1,0:T(8,128)(2,1)}, u32[]{:S(2)}) copy-start(bf16[512,512]{1,0:T(8,128)(2,1)} %param.13) | copy-start | bytes 1572868
  11.3 42.6 %all-to-all-start.1 = ((bf16[32,40,896]{2,1,0:T(8,128)(2,1)}), bf16[32,40,896]{2,1,0:T(8,128)(2,1)S(1)}, u32[]{:S(2)}, u32[]{:S(2)}) async-start(bf16[32,40,896]{2,1,0:T(8,128)(2,1)} %bitcast.89), calls=%async_computation.1 | async-start | bytes 4587520 | tf_op jit(solution)/shard_map/all_to_all | solution.py:623
  23.0 9.6 %copy-start.10 = (bf16[512]{0:T(512)(128)(2,1)S(1)}, bf16[512]{0:T(512)(128)(2,1)}, u32[]{:S(2)}) copy-start(bf16[512]{0:T(512)(128)(2,1)} %param.15) | copy-start | bytes 3076
  28.1 4.5 %collective-permute-start.2 = (f32[2,512]{1,0:T(2,128)S(1)}, f32[2,512]{1,0:T(2,128)S(1)}, u32[]{:S(2)}, u32[]{:S(2)}) collective-permute-start(f32[2,512]{1,0:T(2,128)S(1)} %pad_maximum_fusion.1), channel_id=1, source_target_pairs={{0,3},{1,0},{2,1},{3,2},{4,7},{5,4},{6,5},{7,6},{8,11},{9,8},{10,9... | collective-permute-start | bytes 12296 | tf_op jit(solution)/shard_map/ppermute | solution.py:19
  30.9 5.1 %collective-permute-start.3 = (f32[2,512]{1,0:T(2,128)S(1)}, f32[2,512]{1,0:T(2,128)S(1)}, u32[]{:S(2)}, u32[]{:S(2)}) collective-permute-start(f32[2,512]{1,0:T(2,128)S(1)} %pad_maximum_fusion.1), channel_id=1, source_target_pairs={{0,2},{1,3},{2,0},{3,1},{4,6},{5,7},{6,4},{7,5},{8,10},{9,11},{10,... | collective-permute-start | bytes 12296 | tf_op jit(solution)/shard_map/ppermute | solution.py:19
  31.7 4.8 %collective-permute-start.1 = (f32[2,512]{1,0:T(2,128)S(1)}, f32[2,512]{1,0:T(2,128)S(1)}, u32[]{:S(2)}, u32[]{:S(2)}) collective-permute-start(f32[2,512]{1,0:T(2,128)S(1)} %pad_maximum_fusion.1), channel_id=1, source_target_pairs={{0,1},{1,2},{2,3},{3,0},{4,5},{5,6},{6,7},{7,4},{8,9},{9,10},{10,1... | collective-permute-start | bytes 12296 | tf_op jit(solution)/shard_map/ppermute | solution.py:19
  53.8 9.4 %copy-start = (bf16[32,40,896]{2,1,0:T(8,128)(2,1)}, bf16[32,40,896]{2,1,0:T(8,128)(2,1)S(1)}, u32[]{:S(2)}) copy-start(bf16[32,40,896]{2,1,0:T(8,128)(2,1)S(1)} %all-to-all-done.1) | copy-start | bytes 6881284
  53.8 59.5 %all-to-all-start = ((bf16[32,40,1408]{2,1,0:T(8,128)(2,1)}), bf16[32,40,1408]{2,1,0:T(8,128)(2,1)}, u32[]{:S(2)}, u32[]{:S(2)}) async-start(bf16[32,40,1408]{2,1,0:T(8,128)(2,1)} %bitcast.82), calls=%async_computation | async-start | bytes 7208960 | tf_op jit(solution)/shard_map/all_to_all | solution.py:623
  60.0 42.0 %collective-permute-start.13 = (bf16[960,896]{1,0:T(8,128)(2,1)}, bf16[960,896]{1,0:T(8,128)(2,1)}, u32[]{:S(2)}, u32[]{:S(2)}) collective-permute-start(bf16[960,896]{1,0:T(8,128)(2,1)} %bitcast.48), channel_id=1, source_target_pairs={{0,1},{1,2},{2,3},{3,0},{4,5},{5,6},{6,7},{7,4},{8,9},{9,10},{10,1... | collective-permute-start | bytes 5160968 | tf_op jit(solution)/shard_map/ppermute | solution.py:19
  61.5 40.7 %collective-permute-start.12 = (bf16[960,896]{1,0:T(8,128)(2,1)}, bf16[960,896]{1,0:T(8,128)(2,1)}, u32[]{:S(2)}, u32[]{:S(2)}) collective-permute-start(bf16[960,896]{1,0:T(8,128)(2,1)} %bitcast.48), channel_id=1, source_target_pairs={{0,3},{1,0},{2,1},{3,2},{4,7},{5,4},{6,5},{7,6},{8,11},{9,8},{10,9... | collective-permute-start | bytes 5160968 | tf_op jit(solution)/shard_map/ppermute | solution.py:19
  63.3 50.0 %collective-permute-start.11 = (bf16[320,896]{1,0:T(8,128)(2,1)S(1)}, bf16[320,896]{1,0:T(8,128)(2,1)S(1)}, u32[]{:S(2)}, u32[]{:S(2)}) collective-permute-start(bf16[320,896]{1,0:T(8,128)(2,1)S(1)} %bitcast.92), channel_id=1, source_target_pairs={{0,1},{1,2},{2,3},{3,0},{4,5},{5,6},{6,7},{7,4},{8,9},{9,10},{10,1... | collective-permute-start | bytes 1720328 | tf_op jit(solution)/shard_map/ppermute | solution.py:19
  63.7 49.6 %collective-permute-start.10 = (bf16[320,896]{1,0:T(8,128)(2,1)S(1)}, bf16[320,896]{1,0:T(8,128)(2,1)S(1)}, u32[]{:S(2)}, u32[]{:S(2)}) collective-permute-start(bf16[320,896]{1,0:T(8,128)(2,1)S(1)} %bitcast.93), channel_id=1, source_target_pairs={{0,3},{1,0},{2,1},{3,2},{4,7},{5,4},{6,5},{7,6},{8,11},{9,8},{10,9... | collective-permute-start | bytes 1720328 | tf_op jit(solution)/shard_map/ppermute | solution.py:19
  113.3 0.8 copy-start.5
  113.3 1.0 copy-start.6
  135.5 55.9 %all-to-all-start.2 = ((bf16[32,40,1024]{2,1,0:T(8,128)(2,1)}), bf16[32,40,1024]{2,1,0:T(8,128)(2,1)S(1)}, u32[]{:S(2)}, u32[]{:S(2)}) async-start(bf16[32,40,1024]{2,1,0:T(8,128)(2,1)} %bitcast.83), calls=%async_computation.2 | async-start | bytes 5242880 | tf_op jit(solution)/shard_map/all_to_all | solution.py:623
  147.1 33.2 %collective-permute-start.17 = (bf16[320,2048]{1,0:T(8,128)(2,1)}, bf16[320,2048]{1,0:T(8,128)(2,1)}, u32[]{:S(2)}, u32[]{:S(2)}) collective-permute-start(bf16[320,2048]{1,0:T(8,128)(2,1)} %get-tuple-element.54), channel_id=1, source_target_pairs={{0,1},{1,2},{2,3},{3,0},{4,5},{5,6},{6,7},{7,4},{8,9},{9,10},{10,1... | collective-permute-start | bytes 3932168 | tf_op jit(solution)/shard_map/ppermute | solution.py:19
  148.4 33.4 %collective-permute-start.18 = (bf16[320,2048]{1,0:T(8,128)(2,1)}, bf16[320,2048]{1,0:T(8,128)(2,1)}, u32[]{:S(2)}, u32[]{:S(2)}) collective-permute-start(bf16[320,2048]{1,0:T(8,128)(2,1)} %get-tuple-element.55), channel_id=1, source_target_pairs={{0,3},{1,0},{2,1},{3,2},{4,7},{5,4},{6,5},{7,6},{8,11},{9,8},{10,9... | collective-permute-start | bytes 3932168 | tf_op jit(solution)/shard_map/ppermute | solution.py:19
  150.3 41.1 %collective-permute-start.4 = (bf16[128,2048]{1,0:T(8,128)(2,1)}, bf16[128,2048]{1,0:T(8,128)(2,1)S(1)}, u32[]{:S(2)}, u32[]{:S(2)}) collective-permute-start(bf16[128,2048]{1,0:T(8,128)(2,1)} %get-tuple-element.39), channel_id=1, source_target_pairs={{0,1},{1,2},{2,3},{3,0},{4,5},{5,6},{6,7},{7,4},{8,9},{9,10},{10,1... | collective-permute-start | bytes 1572872 | tf_op jit(solution)/shard_map/ppermute | solution.py:19
  154.5 65.0 %collective-permute-start.14 = (bf16[320,2048]{1,0:T(8,128)(2,1)}, bf16[320,2048]{1,0:T(8,128)(2,1)}, u32[]{:S(2)}, u32[]{:S(2)}) collective-permute-start(bf16[320,2048]{1,0:T(8,128)(2,1)} %get-tuple-element.51), channel_id=1, source_target_pairs={{0,1},{1,2},{2,3},{3,0},{4,5},{5,6},{6,7},{7,4},{8,9},{9,10},{10,1... | collective-permute-start | bytes 3932168 | tf_op jit(solution)/shard_map/ppermute | solution.py:19
  156.6 89.4 %collective-permute-start.6 = (bf16[128,2048]{1,0:T(8,128)(2,1)}, bf16[128,2048]{1,0:T(8,128)(2,1)}, u32[]{:S(2)}, u32[]{:S(2)}) collective-permute-start(bf16[128,2048]{1,0:T(8,128)(2,1)} %get-tuple-element.40), channel_id=1, source_target_pairs={{0,3},{1,0},{2,1},{3,2},{4,7},{5,4},{6,5},{7,6},{8,11},{9,8},{10,9... | collective-permute-start | bytes 1572872 | tf_op jit(solution)/shard_map/ppermute | solution.py:19
  180.2 22.9 %collective-permute-start.7 = (bf16[128,2048]{1,0:T(8,128)(2,1)}, bf16[128,2048]{1,0:T(8,128)(2,1)}, u32[]{:S(2)}, u32[]{:S(2)}) collective-permute-start(bf16[128,2048]{1,0:T(8,128)(2,1)} %get-tuple-element.42), channel_id=1, source_target_pairs={{0,3},{1,0},{2,1},{3,2},{4,7},{5,4},{6,5},{7,6},{8,11},{9,8},{10,9... | collective-permute-start | bytes 1572872 | tf_op jit(solution)/shard_map/ppermute | solution.py:19
  181.8 49.1 %collective-permute-start.15 = (bf16[320,2048]{1,0:T(8,128)(2,1)}, bf16[320,2048]{1,0:T(8,128)(2,1)}, u32[]{:S(2)}, u32[]{:S(2)}) collective-permute-start(bf16[320,2048]{1,0:T(8,128)(2,1)} %get-tuple-element.52), channel_id=1, source_target_pairs={{0,3},{1,0},{2,1},{3,2},{4,7},{5,4},{6,5},{7,6},{8,11},{9,8},{10,9... | collective-permute-start | bytes 3932168 | tf_op jit(solution)/shard_map/ppermute | solution.py:19
  191.4 0.8 copy-start.8
  191.4 54.7 %collective-permute-start.9 = (bf16[128,2048]{1,0:T(8,128)(2,1)}, bf16[128,2048]{1,0:T(8,128)(2,1)}, u32[]{:S(2)}, u32[]{:S(2)}) collective-permute-start(bf16[128,2048]{1,0:T(8,128)(2,1)} %get-tuple-element.43), channel_id=1, source_target_pairs={{0,1},{1,2},{2,3},{3,0},{4,5},{5,6},{6,7},{7,4},{8,9},{9,10},{10,1... | collective-permute-start | bytes 1572872 | tf_op jit(solution)/shard_map/ppermute | solution.py:19
  192.2 1.5 copy-start.3
  192.2 11.8 %copy-start.7 = (bf16[128,2048]{1,0:T(8,128)(2,1)S(1)}, bf16[128,2048]{1,0:T(8,128)(2,1)}, u32[]{:S(2)}) copy-start(bf16[128,2048]{1,0:T(8,128)(2,1)} %get-tuple-element.41) | copy-start | bytes 1572868
  193.6 41.3 %all-to-all-start.4 = ((bf16[32,40,512]{2,1,0:T(8,128)(2,1)}), bf16[32,40,512]{2,1,0:T(8,128)(2,1)S(1)}, u32[]{:S(2)}, u32[]{:S(2)}) async-start(bf16[32,40,512]{2,1,0:T(8,128)(2,1)} %bitcast.86), calls=%async_computation.4 | async-start | bytes 2621440 | tf_op jit(solution)/shard_map/all_to_all | solution.py:623
  201.0 20.1 %copy-start.11 = (f32[512,2]{0,1:T(2,128)S(1)}, f32[512,2]{0,1:T(2,128)}, u32[]{:S(2)}) copy-start(f32[512,2]{0,1:T(2,128)} %param.20) | copy-start | bytes 12292
  203.2 42.9 %collective-permute-start.5 = (bf16[128,2048]{1,0:T(8,128)(2,1)}, bf16[128,2048]{1,0:T(8,128)(2,1)}, u32[]{:S(2)}, u32[]{:S(2)}) collective-permute-start(bf16[128,2048]{1,0:T(8,128)(2,1)} %add_convert_fusion.3), channel_id=1, source_target_pairs={{0,1},{1,2},{2,3},{3,0},{4,5},{5,6},{6,7},{7,4},{8,9},{9,10},{10,1... | collective-permute-start | bytes 1572872 | tf_op jit(solution)/shard_map/ppermute | solution.py:19
  219.6 26.5 %collective-permute-start.8 = (bf16[128,2048]{1,0:T(8,128)(2,1)}, bf16[128,2048]{1,0:T(8,128)(2,1)S(1)}, u32[]{:S(2)}, u32[]{:S(2)}) collective-permute-start(bf16[128,2048]{1,0:T(8,128)(2,1)} %add_convert_fusion.1), channel_id=1, source_target_pairs={{0,3},{1,0},{2,1},{3,2},{4,7},{5,4},{6,5},{7,6},{8,11},{9,8},{10,9... | collective-permute-start | bytes 1572872 | tf_op jit(solution)/shard_map/ppermute | solution.py:19
  235.0 13.4 %copy-start.2 = (bf16[32,40,512]{2,1,0:T(8,128)(2,1)}, bf16[32,40,512]{2,1,0:T(8,128)(2,1)S(1)}, u32[]{:S(2)}) copy-start(bf16[32,40,512]{2,1,0:T(8,128)(2,1)S(1)} %all-to-all-done.4) | copy-start | bytes 3932164
  235.0 38.7 %all-to-all-start.3 = ((bf16[32,40,512]{2,1,0:T(8,128)(2,1)}), bf16[32,40,512]{2,1,0:T(8,128)(2,1)S(1)}, u32[]{:S(2)}, u32[]{:S(2)}) async-start(bf16[32,40,512]{2,1,0:T(8,128)(2,1)} %bitcast.87), calls=%async_computation.3 | async-start | bytes 2621440 | tf_op jit(solution)/shard_map/all_to_all | solution.py:623
  242.4 27.2 %collective-permute-start.16 = (bf16[128,4096]{1,0:T(8,128)(2,1)}, bf16[128,4096]{1,0:T(8,128)(2,1)}, u32[]{:S(2)}, u32[]{:S(2)}) collective-permute-start(bf16[128,4096]{1,0:T(8,128)(2,1)} %combined.3), channel_id=1, source_target_pairs={{0,2},{1,3},{2,0},{3,1},{4,6},{5,7},{6,4},{7,5},{8,10},{9,11},{10,... | collective-permute-start | bytes 3145736 | tf_op jit(solution)/shard_map/ppermute | solution.py:19
  273.6 1.1 copy-start.1
